TPU v7x, 32 devices: a whole 2x2x4 slice. The times are simulated.
32 devices in a mesh: grp: 2 (over y), sp: 4 (over z), tp: 4 (over x, core).
Axes of the slice: x: 2, y: 2, z: 4, core: 2. Of those that a mesh axis runs over, the one named last changes fastest.
Arguments:
- tokens: bfloat16 [8, 1024, 2048], P('grp', 'sp'), parts along dimension 0, may hold values from -6 to 6
- norm_gain: bfloat16 [2048], replicated, may hold values from 0.099609375 to 1.8984375
- key_weight: bfloat16 [2048, 2048], P(None, 'tp'), may hold values from -0.125 to 0.125
- value_weight: bfloat16 [2048, 2048], P(None, 'tp'), may hold values from -0.125 to 0.125
- break_bias: bfloat16 [8, 1024, 16], P('grp', 'sp', 'tp'), parts along dimension 0, may hold values from -12 to 0
- new_query: bfloat16 [8, 2048], P('grp', 'tp'), parts along dimension 0, may hold values from -6 to 6
Outputs:
- cache_pair: bfloat16 [8, 4, 256, 2, 2048], P(('grp', 'sp'), None, None, None, 'tp'), parts along dimension 0
- cache_bias: bfloat16 [8, 4, 256, 16], P(('grp', 'sp'), None, None, 'tp'), parts along dimension 0
- attended: float32 [8, 2048], P('grp', 'tp'), parts along dimension 0
There are 2 independent parts, one for each index of `grp`. A program takes and returns all parts, laid end to end along the dimension named above; an argument that names none is the same for every part. Nothing has to cross between parts.
All inputs are finite; a program needn't handle non-finite values.
Results may differ from a plain program's by a relative error of at most 0.0064.
Values may be sent and summed in bfloat16 or wider, within the bound.
No kernel may reach another device: no remote copies, remote signals or barrier semaphores. Data moves between devices by JAX's collectives and lax.ppermute only.
A program may use at most 64 MiB of HBM per device.

v0:
```python
import jax
import jax.numpy as jnp
from jax import lax
from jax.sharding import PartitionSpec as P

norm_eps = 1e-06


def normalize(tokens, norm_gain):
    widened = tokens.astype(jnp.float32)
    inverse = lax.rsqrt(jnp.mean(widened * widened, axis=-1, keepdims=True) + norm_eps)
    return (widened * inverse * norm_gain.astype(jnp.float32)).astype(jnp.bfloat16)


def project(flat_rows, key_weight, value_weight):
    key_rows = jnp.dot(flat_rows, key_weight, preferred_element_type=jnp.float32).astype(
        jnp.bfloat16
    )
    value_rows = jnp.dot(flat_rows, value_weight, preferred_element_type=jnp.float32).astype(
        jnp.bfloat16
    )
    return (key_rows, value_rows)


def read_placed(new_query, key_rows, value_rows, bias_rows, seq_count):
    block_count, piece, heads_here = bias_rows.shape
    columns = key_rows.shape[2]
    head_size = columns // heads_here
    span = block_count // seq_count
    own_index = lax.axis_index("sp")
    own_seq = own_index // span
    own_part = own_index % span
    own_query = lax.dynamic_slice_in_dim(new_query, own_seq, 1, 0).reshape(heads_here, head_size)
    key_heads = key_rows.reshape(block_count, piece, heads_here, head_size)
    logits = jnp.einsum("hd,nphd->nph", own_query, key_heads, preferred_element_type=jnp.float32)
    logits = logits * head_size ** (-0.5) + bias_rows.astype(jnp.float32)
    keep_log = jax.nn.log_sigmoid(-logits)
    block_totals = jnp.sum(keep_log, axis=1)
    own_slot = (jnp.arange(block_count, dtype=jnp.int32) == own_index)[:, None, None]
    placed = jnp.where(own_slot, block_totals[None], 0.0)
    gathered = lax.psum(placed, "sp")
    same_prompt = lax.dynamic_slice_in_dim(gathered, own_seq * span, span, 0)
    ordered = jnp.transpose(same_prompt, (1, 0, 2)).reshape(block_count * span, heads_here)
    beyond = lax.cumsum(ordered, axis=0, reverse=True) - ordered
    beyond = beyond.reshape(block_count, span, heads_here)
    carried = lax.dynamic_slice_in_dim(beyond, own_part, 1, 1)[:, 0, :]
    later_sum = lax.cumsum(keep_log, axis=1, reverse=True) - keep_log + carried[:, None, :]
    stick_weights = jnp.exp(jax.nn.log_sigmoid(logits) + later_sum).astype(jnp.bfloat16)
    value_heads = value_rows.reshape(block_count, piece, heads_here, head_size)
    mixed = jnp.einsum(
        "nph,nphd->hd", stick_weights, value_heads, preferred_element_type=jnp.float32
    )
    chosen = (jnp.arange(seq_count, dtype=jnp.int32) == own_seq)[:, None]
    partial_rows = jnp.where(chosen, mixed.reshape(1, columns), 0.0)
    return lax.psum(partial_rows, "sp")


def local(tokens, norm_gain, key_weight, value_weight, break_bias, new_query):
    seq_count, tok_rows, width = tokens.shape
    heads_here = break_bias.shape[2]
    block_count = lax.axis_size("sp")
    piece = tok_rows * seq_count // block_count
    columns = key_weight.shape[1]
    normed = normalize(tokens, norm_gain)
    bias_pieces = break_bias.reshape(block_count, piece, heads_here)
    key_rows, value_rows = project(normed.reshape(-1, width), key_weight, value_weight)
    stacked_rows = jnp.stack((key_rows, value_rows), axis=1).reshape(block_count, piece, 2, columns)
    paired, bias_arrived = (
        lax.all_to_all(stacked_rows, "sp", split_axis=0, concat_axis=0, tiled=True),
        lax.all_to_all(bias_pieces, "sp", split_axis=0, concat_axis=0, tiled=True),
    )
    key_rows = paired[:, :, 0]
    value_rows = paired[:, :, 1]
    attended = read_placed(new_query, key_rows, value_rows, bias_arrived, seq_count)
    return (paired[None], bias_arrived[None], attended)


def solution(mesh):
    return jax.shard_map(
        local,
        mesh=mesh,
        in_specs=(
            P("grp", "sp", None),
            P(),
            P(None, "tp"),
            P(None, "tp"),
            P("grp", "sp", "tp"),
            P("grp", "tp"),
        ),
        out_specs=(
            P(("grp", "sp"), None, None, None, "tp"),
            P(("grp", "sp"), None, None, "tp"),
            P("grp", "tp"),
        ),
        check_vma=False,
    )
```

profile of v0, /device:TPU:0, one launch (start us, length us, event | category | flops | bytes accessed | tf_op | source)
XLA Modules:
  0.0 130.2 jit_solution(2703418311215314435)
XLA Ops:
  0.6 0.0 copy-start
  0.6 0.0 copy-start.3
  0.7 6.5 %all-to-all-start.1 = ((bf16[4,256,4]{1,2,0:T(4,128)(2,1)}), bf16[4,256,4]{1,2,0:T(4,128)(2,1)S(1)}, u32[]{:S(2)}, u32[]{:S(2)}) async-start(bf16[4,256,4]{1,2,0:T(4,128)(2,1)} %param.10), calls=%async_computation.1 | async-start | bytes 16384 | tf_op jit(solution)/shard_map/all_to_all | solution.py:70
  7.1 0.0 copy-start.1
  7.1 3.2 %fusion = f32[4,256]{1,0:T(4,128)S(1)} fusion(bf16[4,256,2048]{2,1,0:T(8,128)(2,1)} %param.6), kind=kLoop, calls=%fused_computation.2 | loop fusion | flops 6290432 | bytes 4198400 | tf_op jit(solution)/shard_map/reduce_sum | solution.py:11
  10.4 0.0 copy-done.3
  10.4 0.2 copy-done.1
  10.6 1.0 fusion.2
  11.6 0.0 copy-start.2
  11.6 0.0 copy-done
  11.6 3.3 %convolution_convert_fusion.1 = bf16[1024,512]{1,0:T(8,128)(2,1)} fusion(bf16[1024,2048]{1,0:T(8,128)(2,1)S(1)} %bitcast.69, bf16[2048,512]{1,0:T(8,128)(2,1)S(1)} %copy-done), kind=kOutput, calls=%fused_computation.7 | convolution fusion | flops 2148007936 | bytes 7340032 | tf_op jit(solution)/shard_map/dot_general | solution.py:16
  15.0 0.0 copy-done.2
  15.0 1.5 %copy.18 = bf16[4,256,1,512]{1,3,2,0:T(8,128)(2,1)S(1)} copy(bf16[4,256,1,512]{3,1,0,2:T(8,128)(2,1)} %bitcast.72) | data formatting | bytes 2097152 | tf_op jit(solution)/shard_map/stack | solution.py:67
  16.4 6.2 %convolution_convert_fusion = bf16[1024,512]{1,0:T(8,128)(2,1)} fusion(bf16[1024,2048]{1,0:T(8,128)(2,1)} %bitcast.70, bf16[2048,512]{1,0:T(8,128)(2,1)} %param.9), kind=kOutput, calls=%fused_computation.6 | convolution fusion | flops 2148007936 | bytes 7340032 | tf_op jit(solution)/shard_map/dot_general | solution.py:19
  22.6 2.3 %copy.19 = bf16[4,256,1,512]{1,3,2,0:T(8,128)(2,1)} copy(bf16[4,256,1,512]{3,1,0,2:T(8,128)(2,1)} %bitcast.71) | data formatting | bytes 2097152 | tf_op jit(solution)/shard_map/stack | solution.py:67
  24.9 2.7 %pad_maximum_fusion = bf16[4,256,2,512]{1,3,2,0:T(8,128)(2,1)} fusion(bf16[4,256,1,512]{1,3,2,0:T(8,128)(2,1)} %copy.19, bf16[4,256,1,512]{1,3,2,0:T(8,128)(2,1)S(1)} %copy.18), kind=kLoop, calls=%fused_computation.5 | loop fusion | flops 1048576 | bytes 4194304 | tf_op jit(solution)/shard_map/stack | solution.py:67
  27.6 0.0 copy-start.4
  27.6 0.0 all-to-all-done.1
  27.6 5.2 %all-to-all-start = ((bf16[4,256,2,512]{1,3,2,0:T(8,128)(2,1)}), bf16[4,256,2,512]{1,3,2,0:T(8,128)(2,1)}, u32[]{:S(2)}, u32[]{:S(2)}) async-start(bf16[4,256,2,512]{1,3,2,0:T(8,128)(2,1)} %pad_maximum_fusion), calls=%async_computation | async-start | bytes 4194304 | tf_op jit(solution)/shard_map/all_to_all | solution.py:69
  32.8 47.8 %all-to-all-done = bf16[4,256,2,512]{1,3,2,0:T(8,128)(2,1)} async-done(((bf16[4,256,2,512]{1,3,2,0:T(8,128)(2,1)}), bf16[4,256,2,512]{1,3,2,0:T(8,128)(2,1)}, u32[]{:S(2)}, u32[]{:S(2)}) %all-to-all-start) | async-done | bytes 2097184 | tf_op jit(solution)/shard_map/all_to_all | solution.py:69
  80.6 1.7 %fusion.20 = (bf16[4,256,1,512]{1,3,2,0:T(8,128)(2,1)S(1)}, bf16[4,256,1,512]{1,3,2,0:T(8,128)(2,1)S(1)}) fusion(bf16[4,256,2,512]{1,3,2,0:T(8,128)(2,1)} %all-to-all-done), kind=kLoop, calls=%fused_computation.37 | loop fusion | bytes 4194304 | tf_op jit(solution)/shard_map/slice | solution.py:72
  82.3 0.0 copy-done.4
  82.3 0.2 fusion.5
  82.5 0.1 negate_bitcast_fusion
  82.7 0.1 broadcast_select_fusion.1
  82.7 10.0 %psum.14 = f32[4,4,4]{2,1,0:T(4,128)S(1)} all-reduce(f32[4,4,4]{2,1,0:T(4,128)S(1)} %broadcast_select_fusion.1), channel_id=1, replica_groups=mesh['grp'=2,'sp'=4,'tp'=4] {'sp'}, use_global_device_ids=true, to_apply=%region_4.5 | all-reduce | flops 64 | bytes 512 | tf_op jit(solution)/shard_map/psum | solution.py:41
  92.8 20.1 %reduce-window.6 = f32[4,4,2,128]{3,2,1,0:T(2,128)S(1)} reduce-window(f32[4,4,2,128]{3,2,1,0:T(2,128)S(1)} %reshape.54, f32[]{:T(128)} %constant.36.clone.1), window={size=1x1x1x128 pad=0_0x0_0x0_0x0_127}, to_apply=%region_1.2 | reduce-window | flops 520192 | bytes 32772 | tf_op jit(solution)/shard_map/reduce-window
  112.9 0.1 copy.21
  113.1 0.1 copy.22
  113.2 0.1 broadcast_add_fusion
  113.3 0.1 fusion.13
  113.4 0.4 fusion.3
  113.8 0.1 broadcast_select_fusion
  113.8 9.6 %psum.15 = f32[4,512]{1,0:T(4,128)} all-reduce(f32[4,512]{1,0:T(4,128)S(1)} %broadcast_select_fusion), channel_id=1, replica_groups=mesh['grp'=2,'sp'=4,'tp'=4] {'sp'}, use_global_device_ids=true, to_apply=%region_6.7 | all-reduce | flops 2048 | bytes 16384 | tf_op jit(solution)/shard_map/psum | solution.py:55
  123.5 6.2 %copy.24 = bf16[1,4,256,2,512]{4,3,2,1,0:T(2,128)(2,1)} copy(bf16[1,4,256,2,512]{2,4,3,1,0:T(8,128)(2,1)} %bitcast.3) | data formatting | bytes 4194304
  129.6 0.6 copy.51
  (11 shorter events, 0.1 us)
Async XLA Ops:
  0.6 11.0 %copy-start = (bf16[2048,512]{1,0:T(8,128)(2,1)S(1)}, bf16[2048,512]{1,0:T(8,128)(2,1)}, u32[]{:S(2)}) copy-start(bf16[2048,512]{1,0:T(8,128)(2,1)} %param.8) | copy-start | bytes 6291460
  0.6 9.7 %copy-start.3 = (bf16[2048]{0:T(1024)(128)(2,1)S(1)}, bf16[2048]{0:T(1024)(128)(2,1)}, u32[]{:S(2)}) copy-start(bf16[2048]{0:T(1024)(128)(2,1)} %param.7) | copy-start | bytes 12292
  0.7 27.0 %all-to-all-start.1 = ((bf16[4,256,4]{1,2,0:T(4,128)(2,1)}), bf16[4,256,4]{1,2,0:T(4,128)(2,1)S(1)}, u32[]{:S(2)}, u32[]{:S(2)}) async-start(bf16[4,256,4]{1,2,0:T(4,128)(2,1)} %param.10), calls=%async_computation.1 | async-start | bytes 16384 | tf_op jit(solution)/shard_map/all_to_all | solution.py:70
  7.1 3.4 %copy-start.1 = (bf16[4,256,2048]{2,1,0:T(8,128)(2,1)S(1)}, bf16[4,256,2048]{2,1,0:T(8,128)(2,1)}, u32[]{:S(2)}) copy-start(bf16[4,256,2048]{2,1,0:T(8,128)(2,1)} %param.6) | copy-start | bytes 12582916
  11.6 3.3 %copy-start.2 = (bf16[4,256,2048]{2,1,0:T(8,128)(2,1)}, bf16[4,256,2048]{2,1,0:T(8,128)(2,1)S(1)}, u32[]{:S(2)}) copy-start(bf16[4,256,2048]{2,1,0:T(8,128)(2,1)S(1)} %fusion.2) | copy-start | bytes 12582916
  27.6 54.7 %copy-start.4 = (bf16[4,512]{1,0:T(4,128)(2,1)S(1)}, bf16[4,512]{1,0:T(4,128)(2,1)}, u32[]{:S(2)}) copy-start(bf16[4,512]{1,0:T(4,128)(2,1)} %param.11) | copy-start | bytes 12292
  27.6 53.0 %all-to-all-start = ((bf16[4,256,2,512]{1,3,2,0:T(8,128)(2,1)}), bf16[4,256,2,512]{1,3,2,0:T(8,128)(2,1)}, u32[]{:S(2)}, u32[]{:S(2)}) async-start(bf16[4,256,2,512]{1,3,2,0:T(8,128)(2,1)} %pad_maximum_fusion), calls=%async_computation | async-start | bytes 4194304 | tf_op jit(solution)/shard_map/all_to_all | solution.py:69
where the time goes:
time: 131 us; the launch traced here: 130 us
  waiting for transfers between devices  47.8 us (36%)
  other arithmetic  27.6 us (21%)
  blocking collectives  19.6 us (15%)
  local copies, waits for them, and re-layouts  12.7 us (10%)
  starting transfers between devices  11.7 us (9%)
  matrix products  10.1 us (8%)
    all_to_all x1, waiting for transfers between devices, local(): lax.all_to_all(stacked_rows, 'sp', split_axis=0, concat_axis=0, tiled=True)  47.8 us
    another operation x2, other arithmetic  20.1 us
    psum x1, blocking collectives, read_placed(): gathered = lax.psum(placed, 'sp')  9.95 us
    psum x1, blocking collectives, read_placed(): return lax.psum(partial_rows, 'sp')  9.64 us
    unnamed x12, local copies, waits for them, and re-layouts  6.96 us
    all_to_all x1, starting transfers between devices, local(): lax.all_to_all(bias_pieces, 'sp', split_axis=0, concat_axis=0, tiled=True)  6.49 us
    dot_general x1, matrix products, project(): jnp.dot(flat_rows, value_weight, preferred_element_type=jnp.float32)  6.16 us
    all_to_all x1, starting transfers between devices, local(): lax.all_to_all(stacked_rows, 'sp', split_axis=0, concat_axis=0, tiled=True)  5.22 us
  transfers between devices with their start and end apart: 2, of which 1 were waited for; matrix products, arithmetic and copies ran while one was open for 16% of the time, Pallas kernels for 0%

commit v1 on v0

--- a/solution.py
+++ b/solution.py
@@ -1,6 +1,10 @@
+import functools
+
 import jax
 import jax.numpy as jnp
 from jax import lax
+from jax.experimental import pallas as pl
+from jax.experimental.pallas import tpu as pltpu
 from jax.sharding import PartitionSpec as P
 
 norm_eps = 1e-06
@@ -55,7 +59,7 @@
     return lax.psum(partial_rows, "sp")
 
 
-def local(tokens, norm_gain, key_weight, value_weight, break_bias, new_query):
+def exchange_rows(tokens, norm_gain, key_weight, value_weight, break_bias, new_query):
     seq_count, tok_rows, width = tokens.shape
     heads_here = break_bias.shape[2]
     block_count = lax.axis_size("sp")
@@ -73,6 +77,205 @@
     value_rows = paired[:, :, 1]
     attended = read_placed(new_query, key_rows, value_rows, bias_arrived, seq_count)
     return (paired[None], bias_arrived[None], attended)
+
+
+def block_kernel(part_count, whole_rows, carried, *refs):
+    index_ref = refs[0]
+    parts = refs[1 : 1 + part_count]
+    gain_ref, key_ref, value_ref, bias_ref, query_ref = refs[1 + part_count : 6 + part_count]
+    rest = refs[6 + part_count + (2 if carried else 0) :]
+    cache_ref, bias_out_ref, partial_ref, total_ref, normed_ref = rest
+    piece, width = normed_ref.shape
+    heads_here = bias_ref.shape[-2]
+    columns = key_ref.shape[1]
+    head_size = columns // heads_here
+    gain = gain_ref[...].astype(jnp.float32)
+    if whole_rows:
+        widened = parts[0][0].astype(jnp.float32)
+        square_sum = jnp.sum(widened * widened, axis=-1, keepdims=True)
+        inverse = lax.rsqrt(square_sum * (1.0 / width) + norm_eps)
+        normed_ref[...] = (widened * inverse * gain).astype(jnp.bfloat16)
+    else:
+        share = width // part_count
+        square_sum = jnp.zeros((piece, 1), jnp.float32)
+        for part in parts:
+            widened = part[...].astype(jnp.float32)
+            square_sum = square_sum + jnp.sum(widened * widened, axis=-1, keepdims=True)
+        inverse = lax.rsqrt(square_sum * (1.0 / width) + norm_eps)
+        for offset, part in enumerate(parts):
+            start = pl.multiple_of((index_ref[1] ^ offset) * share, share)
+            own_gain = gain_ref[:, pl.ds(start, share)].astype(jnp.float32)
+            scaled = part[...].astype(jnp.float32) * inverse * own_gain
+            normed_ref[:, pl.ds(start, share)] = scaled.astype(jnp.bfloat16)
+    normed = normed_ref[...]
+    key_rows = jnp.dot(normed, key_ref[...], preferred_element_type=jnp.float32).astype(
+        jnp.bfloat16
+    )
+    value_rows = jnp.dot(normed, value_ref[...], preferred_element_type=jnp.float32).astype(
+        jnp.bfloat16
+    )
+    cache_ref[0, 0] = jnp.stack((key_rows, value_rows), axis=1)
+    bias = bias_ref[...].reshape(heads_here, piece)
+    bias_out_ref[0] = bias
+    head_of_row = lax.broadcasted_iota(jnp.int32, (heads_here, columns), 0)
+    head_of_column = lax.broadcasted_iota(jnp.int32, (heads_here, columns), 1) // head_size
+    own_head = head_of_row == head_of_column
+    query = jnp.where(own_head, query_ref[...], 0.0).astype(jnp.bfloat16)
+    logits = lax.dot_general(
+        query, key_rows, (((1,), (1,)), ((), ())), preferred_element_type=jnp.float32
+    )
+    logits = logits * head_size ** (-0.5) + bias.astype(jnp.float32)
+    soft = jnp.log1p(jnp.exp(-jnp.abs(logits)))
+    keep_log = jnp.minimum(-logits, 0.0) - soft
+    break_log = jnp.minimum(logits, 0.0) - soft
+    earlier = lax.broadcasted_iota(jnp.int32, (piece, piece), 1)
+    later = lax.broadcasted_iota(jnp.int32, (piece, piece), 0) > earlier
+    later_sum = jnp.dot(
+        keep_log,
+        later.astype(jnp.float32),
+        preferred_element_type=jnp.float32,
+        precision=lax.Precision.HIGHEST,
+    )
+    weights = jnp.exp(break_log + later_sum).astype(jnp.bfloat16)
+    mixed = jnp.dot(weights, value_rows, preferred_element_type=jnp.float32)
+    partial_ref[...] = jnp.sum(jnp.where(own_head, mixed, 0.0), axis=0, keepdims=True)
+    totals = jnp.sum(keep_log, axis=1, keepdims=True)
+    total_ref[...] = jnp.sum(jnp.where(own_head, totals, 0.0), axis=0, keepdims=True)
+
+
+def build_block(index, parts, gain, key_weight, value_weight, bias, query, carried, block_count):
+    whole_rows = parts[0].ndim == 3
+    width, columns = key_weight.shape
+    piece = parts[0].shape[-2]
+    heads_here = bias.shape[-2]
+    part_count = len(parts)
+
+    def full(array):
+        return pl.BlockSpec(array.shape, lambda g, s: (0,) * array.ndim)
+
+    if whole_rows:
+        part_specs = [pl.BlockSpec((1, piece, width), lambda g, s: (s[0], 0, 0))]
+        bias_spec = pl.BlockSpec((1, heads_here, piece), lambda g, s: (s[0], 0, 0))
+    else:
+        part_specs = [full(part) for part in parts]
+        bias_spec = full(bias)
+    operands = [index, *parts, gain, key_weight, value_weight, bias, query]
+    specs = part_specs + [full(gain), full(key_weight), full(value_weight), bias_spec, full(query)]
+    aliases = {}
+    if carried is not None:
+        aliases = {len(operands): 0, len(operands) + 1: 1}
+        operands += list(carried)
+        specs += [pl.BlockSpec(memory_space=pl.ANY)] * 2
+    row = jax.ShapeDtypeStruct((1, columns), jnp.float32)
+    return pl.pallas_call(
+        functools.partial(block_kernel, part_count, whole_rows, carried is not None),
+        grid_spec=pltpu.PrefetchScalarGridSpec(
+            num_scalar_prefetch=1,
+            grid=(1,),
+            in_specs=specs,
+            out_specs=[
+                pl.BlockSpec((1, 1, piece, 2, columns), lambda g, s: (0, s[0], 0, 0, 0)),
+                pl.BlockSpec((1, heads_here, piece), lambda g, s: (s[0], 0, 0)),
+                pl.BlockSpec((1, columns), lambda g, s: (0, 0)),
+                pl.BlockSpec((1, columns), lambda g, s: (0, 0)),
+            ],
+            scratch_shapes=[pltpu.VMEM((piece, width), jnp.bfloat16)],
+        ),
+        out_shape=[
+            jax.ShapeDtypeStruct((1, block_count, piece, 2, columns), jnp.bfloat16),
+            jax.ShapeDtypeStruct((block_count, heads_here, piece), jnp.bfloat16),
+            row,
+            row,
+        ],
+        input_output_aliases=aliases,
+    )(*operands)
+
+
+def swap(array, axis, offset):
+    size = lax.axis_size(axis)
+    return lax.ppermute(array, axis, [(k, k ^ offset) for k in range(size)])
+
+
+def exchange_order(size):
+    return [1] + list(range(size - 1, 1, -1))
+
+
+def exchange_tokens(tokens, norm_gain, key_weight, value_weight, break_bias, new_query):
+    seq_count, piece, width = tokens.shape
+    block_count = lax.axis_size("sp")
+    share_count = lax.axis_size("tp")
+    share = width // share_count
+    own = lax.axis_index("sp")
+    own_share = lax.axis_index("tp")
+    bias_rows = jnp.transpose(break_bias, (0, 2, 1))
+    heads_here = bias_rows.shape[1]
+    columns = key_weight.shape[1]
+    gain = norm_gain.reshape(1, width)
+    query = lax.dynamic_slice_in_dim(new_query, own, 1, 0).astype(jnp.float32)
+
+    def index_of(offset):
+        return jnp.stack((own ^ offset, own_share)).astype(jnp.int32)
+
+    order = exchange_order(block_count)
+    arrived = {}
+    bias_arrived = {}
+    for offset in order:
+        sent = lax.dynamic_slice(
+            tokens, (own ^ offset, 0, own_share * share), (1, piece, share)
+        ).reshape(piece, share)
+        arrived[offset] = swap(sent, "sp", offset)
+    for offset in order:
+        bias_sent = lax.dynamic_index_in_dim(bias_rows, own ^ offset, 0, False)
+        bias_arrived[offset] = swap(bias_sent, "sp", offset)
+    built = {}
+    built[0] = build_block(
+        index_of(0), [tokens], gain, key_weight, value_weight, bias_rows, query, None, block_count
+    )
+    latest = built[0]
+    for offset in order:
+        shares = {0: arrived[offset]}
+        bit = share_count // 2
+        while bit:
+            for known in list(shares):
+                shares[known | bit] = swap(shares[known], "tp", bit)
+            bit //= 2
+        parts = [shares[k] for k in range(share_count)]
+        latest = build_block(
+            index_of(offset),
+            parts,
+            gain,
+            key_weight,
+            value_weight,
+            bias_arrived[offset],
+            query,
+            latest[:2],
+            block_count,
+        )
+        built[offset] = latest
+    cache_pair, cache_bias = latest[:2]
+    attended = jnp.zeros((1, columns), jnp.float32)
+    for offset, block in built.items():
+        beyond = jnp.zeros((1, columns), jnp.float32)
+        for other, other_block in built.items():
+            if other != offset:
+                beyond = beyond + jnp.where((own ^ other) > (own ^ offset), other_block[3], 0.0)
+        attended = attended + block[2] * jnp.exp(beyond)
+    seq_index = lax.broadcasted_iota(jnp.int32, (seq_count, 1), 0)
+    gathered = jnp.where(seq_index == own, attended, 0.0)
+    for offset in order:
+        gathered = jnp.where(seq_index == (own ^ offset), swap(attended, "sp", offset), gathered)
+    return (cache_pair, jnp.transpose(cache_bias, (0, 2, 1))[None], gathered)
+
+
+def local(tokens, norm_gain, key_weight, value_weight, break_bias, new_query):
+    seq_count, _, width = tokens.shape
+    block_count = lax.axis_size("sp")
+    share_count = lax.axis_size("tp")
+    paired = block_count & (block_count - 1) == 0 and share_count & (share_count - 1) == 0
+    aligned = width % (128 * share_count) == 0
+    whole_prompt = seq_count == block_count and block_count > 1
+    body = exchange_tokens if paired and aligned and whole_prompt else exchange_rows
+    return body(tokens, norm_gain, key_weight, value_weight, break_bias, new_query)
 
 
 def solution(mesh):

time: 131 us -> 82.5 us (0.63)
  Pallas kernels: 0 us -> 27 us
  waiting for transfers between devices: 47.8 us -> 22.4 us
  other arithmetic: 27.6 us -> 5.07 us
  blocking collectives: 19.6 us -> 0 us
  starting transfers between devices: 11.7 us -> 22 us
  matrix products: 10.1 us -> 0 us
  local copies, waits for them, and re-layouts: 12.7 us -> 4.83 us
    all_to_all x2 -> x0, waiting for transfers between devices: 47.8 us -> none  [the longest x1 47.8 us: local(): lax.all_to_all(stacked_rows, 'sp', split_axis=0, concat_axis=0, tiled=True)]
    pallas_call x0 -> x4, Pallas kernels: none -> 27 us  [build_block(): pl.pallas_call(functools.partial(block_kernel, part_count, whole_rows, ca...]
    ppermute x0 -> x18, waiting for transfers between devices: none -> 22.4 us  [swap(): return lax.ppermute(array, axis, [(k, k ^ offset) for k in range(size)])]
    ppermute x0 -> x18, starting transfers between devices: none -> 22 us  [swap(): return lax.ppermute(array, axis, [(k, k ^ offset) for k in range(size)])]
    another operation x5 -> x4, other arithmetic: 23 us -> 2.4 us  [index_of(): return jnp.stack((own ^ offset, own_share)).astype(jnp.int32)]
    psum x2 -> x0, blocking collectives: 19.6 us -> none  [the longest x1 9.95 us: read_placed(): gathered = lax.psum(placed, 'sp')]
    all_to_all x2 -> x0, starting transfers between devices: 11.7 us -> none  [the longest x1 6.49 us: local(): lax.all_to_all(bias_pieces, 'sp', split_axis=0, concat_axis=0, tiled=True)]
    dot_general x4 -> x0, matrix products: 10.1 us -> none  [the longest x1 6.16 us: project(): jnp.dot(flat_rows, value_weight, preferred_element_type=jnp.float32)]
  transfers between devices with their start and end apart: 2 -> 18, of which waited for: 1 -> 6; matrix products, arithmetic and copies ran while one was open for 16% -> 7% of each run, Pallas kernels for 0% -> 25%
where the time goes in v1:
time: 82.5 us; the launch traced here: 82.2 us
  Pallas kernels  27 us (33%)
  waiting for transfers between devices  22.4 us (27%)
  starting transfers between devices  22 us (27%)
  other arithmetic  5.07 us (6%)
  local copies, waits for them, and re-layouts  4.83 us (6%)
  between operations  0.89 us (1%)
    pallas_call x4, Pallas kernels, build_block(): pl.pallas_call(functools.partial(block_kernel, part_count, whole_rows, ca...  27 us
    ppermute x18, waiting for transfers between devices, swap(): return lax.ppermute(array, axis, [(k, k ^ offset) for k in range(size)])  22.4 us
    ppermute x18, starting transfers between devices, swap(): return lax.ppermute(array, axis, [(k, k ^ offset) for k in range(size)])  22 us
    another operation x4, other arithmetic, index_of(): return jnp.stack((own ^ offset, own_share)).astype(jnp.int32)  2.4 us
  transfers between devices with their start and end apart: 18, of which 6 were waited for; matrix products, arithmetic and copies ran while one was open for 7% of the time, Pallas kernels for 25%

profile of v1, /device:TPU:0, one launch (start us, length us, event | category | flops | bytes accessed | tf_op | source)
XLA Modules:
  0.0 82.2 jit_solution(2741659682977214785)
XLA Ops:
  0.7 1.2 %dynamic-slice_bitcast_fusion = (bf16[256,512]{1,0:T(8,128)(2,1)S(1)}, bf16[256,512]{1,0:T(8,128)(2,1)S(1)}, bf16[256,512]{1,0:T(8,128)(2,1)S(1)}) fusion(bf16[4,256,2048]{2,1,0:T(8,128)(2,1)} %refs_1_.1, s32[]{:T(128)S(6)} %select_n.113, s32[]{:T(128)S(6)} %select_n.110, s32[]{:T(128)S(6)} %select_n.112, s32[]{:T(128)S(6)} %select_n.109), kind=kLoop, calls=%fused_computation | loop fusion | bytes 1572880 | tf_op jit(solution)/shard_map/reshape | solution.py:225
  1.8 3.1 %collective-permute-start.10 = (bf16[256,512]{1,0:T(8,128)(2,1)S(1)}, bf16[256,512]{1,0:T(8,128)(2,1)S(1)}, u32[]{:S(2)}, u32[]{:S(2)}) collective-permute-start(bf16[256,512]{1,0:T(8,128)(2,1)S(1)} %get-tuple-element.35), channel_id=1, source_target_pairs={{0,4},{4,0},{8,12},{12,8},{1,5},{5,1},{9,13},{13,9},{2,6},{6,2},{1... | collective-permute-start | bytes 786440 | tf_op jit(solution)/shard_map/ppermute | solution.py:196
  5.0 2.5 %collective-permute-start.5 = (bf16[256,512]{1,0:T(8,128)(2,1)S(1)}, bf16[256,512]{1,0:T(8,128)(2,1)S(1)}, u32[]{:S(2)}, u32[]{:S(2)}) collective-permute-start(bf16[256,512]{1,0:T(8,128)(2,1)S(1)} %get-tuple-element.36), channel_id=1, source_target_pairs={{0,12},{4,8},{8,4},{12,0},{1,13},{5,9},{9,5},{13,1},{2,14},{6,10},... | collective-permute-start | bytes 786440 | tf_op jit(solution)/shard_map/ppermute | solution.py:196
  7.4 0.1 collective-permute-start
  7.5 4.1 %collective-permute-done.10.refs_1_ = bf16[256,512]{1,0:T(8,128)(2,1)S(1)} collective-permute-done((bf16[256,512]{1,0:T(8,128)(2,1)S(1)}, bf16[256,512]{1,0:T(8,128)(2,1)S(1)}, u32[]{:S(2)}, u32[]{:S(2)}) %collective-permute-start.10) | collective-permute-done | bytes 262176 | tf_op jit(solution)/shard_map/ppermute | solution.py:196
  11.7 1.5 %collective-permute-start.12 = (bf16[256,512]{1,0:T(8,128)(2,1)S(1)}, bf16[256,512]{1,0:T(8,128)(2,1)S(1)}, u32[]{:S(2)}, u32[]{:S(2)}) collective-permute-start(bf16[256,512]{1,0:T(8,128)(2,1)S(1)} %collective-permute-done.10.refs_1_), channel_id=1, source_target_pairs={{0,2},{1,3},{2,0},{3,1},{4,6},{5,7},{6,4},{7,5},{8,10},{9,11},{10,... | collective-permute-start | bytes 786440 | tf_op jit(solution)/shard_map/ppermute | solution.py:196
  13.1 0.7 dynamic-slice_bitcast_fusion.3
  13.9 2.5 %collective-permute-start.14 = (bf16[4,256]{1,0:T(4,128)(2,1)S(1)}, bf16[4,256]{1,0:T(4,128)(2,1)S(1)}, u32[]{:S(2)}, u32[]{:S(2)}) collective-permute-start(bf16[4,256]{1,0:T(4,128)(2,1)S(1)} %get-tuple-element.38), channel_id=1, source_target_pairs={{0,4},{4,0},{8,12},{12,8},{1,5},{5,1},{9,13},{13,9},{2,6},{6,2},{1... | collective-permute-start | bytes 6152 | tf_op jit(solution)/shard_map/ppermute | solution.py:196
  16.3 0.0 collective-permute-start.11
  16.3 4.0 %collective-permute-done.5.refs_1_ = bf16[256,512]{1,0:T(8,128)(2,1)S(1)} collective-permute-done((bf16[256,512]{1,0:T(8,128)(2,1)S(1)}, bf16[256,512]{1,0:T(8,128)(2,1)S(1)}, u32[]{:S(2)}, u32[]{:S(2)}) %collective-permute-start.5) | collective-permute-done | bytes 262176 | tf_op jit(solution)/shard_map/ppermute | solution.py:196
  20.3 1.5 %collective-permute-start.7 = (bf16[256,512]{1,0:T(8,128)(2,1)S(1)}, bf16[256,512]{1,0:T(8,128)(2,1)S(1)}, u32[]{:S(2)}, u32[]{:S(2)}) collective-permute-start(bf16[256,512]{1,0:T(8,128)(2,1)S(1)} %collective-permute-done.5.refs_1_), channel_id=1, source_target_pairs={{0,2},{1,3},{2,0},{3,1},{4,6},{5,7},{6,4},{7,5},{8,10},{9,11},{10,... | collective-permute-start | bytes 786440 | tf_op jit(solution)/shard_map/ppermute | solution.py:196
  21.8 8.6 %collective-permute-done.refs_1_ = bf16[256,512]{1,0:T(8,128)(2,1)S(1)} collective-permute-done((bf16[256,512]{1,0:T(8,128)(2,1)S(1)}, bf16[256,512]{1,0:T(8,128)(2,1)S(1)}, u32[]{:S(2)}, u32[]{:S(2)}) %collective-permute-start) | collective-permute-done | bytes 262176 | tf_op jit(solution)/shard_map/ppermute | solution.py:196
  30.4 1.5 %collective-permute-start.2 = (bf16[256,512]{1,0:T(8,128)(2,1)S(1)}, bf16[256,512]{1,0:T(8,128)(2,1)S(1)}, u32[]{:S(2)}, u32[]{:S(2)}) collective-permute-start(bf16[256,512]{1,0:T(8,128)(2,1)S(1)} %collective-permute-done.refs_1_), channel_id=1, source_target_pairs={{0,2},{1,3},{2,0},{3,1},{4,6},{5,7},{6,4},{7,5},{8,10},{9,11},{10,... | collective-permute-start | bytes 786440 | tf_op jit(solution)/shard_map/ppermute | solution.py:196
  31.9 0.6 pad_add_fusion.3.refs_0_
  32.5 0.0 collective-permute-done.14.refs_8_
  32.5 2.6 %collective-permute-start.9 = (bf16[4,256]{1,0:T(4,128)(2,1)S(1)}, bf16[4,256]{1,0:T(4,128)(2,1)S(1)}, u32[]{:S(2)}, u32[]{:S(2)}) collective-permute-start(bf16[4,256]{1,0:T(4,128)(2,1)S(1)} %get-tuple-element.39), channel_id=1, source_target_pairs={{0,12},{4,8},{8,4},{12,0},{1,13},{5,9},{9,5},{13,1},{2,14},{6,10},... | collective-permute-start | bytes 6152 | tf_op jit(solution)/shard_map/ppermute | solution.py:196
  35.2 0.6 pad_add_fusion.2.refs_0_
  35.7 2.1 %collective-permute-done.9.refs_8_ = bf16[4,256]{1,0:T(4,128)(2,1)S(1)} collective-permute-done((bf16[4,256]{1,0:T(4,128)(2,1)S(1)}, bf16[4,256]{1,0:T(4,128)(2,1)S(1)}, u32[]{:S(2)}, u32[]{:S(2)}) %collective-permute-start.9) | collective-permute-done | bytes 2080 | tf_op jit(solution)/shard_map/ppermute | solution.py:196
  37.9 0.0 collective-permute-start.6
  37.9 0.0 collective-permute-done.11.refs_2_
  37.9 0.5 collective-permute-start.1
  38.4 0.1 collective-permute-start.8
  38.5 0.0 collective-permute-done.2.refs_3_
  38.5 0.4 collective-permute-start.3
  38.9 0.6 pad_add_fusion.1.refs_0_
  39.5 1.3 %dynamic-slice_convert_fusion.refs_6_.refs_9_ = f32[1,512]{1,0:T(1,128)} fusion(bf16[4,512]{1,0:T(4,128)(2,1)} %param.11, s32[]{:T(128)S(6)} %select_n.111), kind=kLoop, calls=%fused_computation.27 | loop fusion | flops 512 | bytes 3076 | tf_op jit(solution)/shard_map/convert_element_type | solution.py:214
  40.8 0.0 collective-permute-done.13.refs_4_
  40.8 1.1 %collective-permute-start.4 = (bf16[4,256]{1,0:T(4,128)(2,1)S(1)}, bf16[4,256]{1,0:T(4,128)(2,1)S(1)}, u32[]{:S(2)}, u32[]{:S(2)}) collective-permute-start(bf16[4,256]{1,0:T(4,128)(2,1)S(1)} %get-tuple-element.40), channel_id=1, source_target_pairs={{0,8},{4,12},{8,0},{12,4},{1,9},{5,13},{9,1},{13,5},{2,10},{6,14},... | collective-permute-start | bytes 6152 | tf_op jit(solution)/shard_map/ppermute | solution.py:196
  41.9 0.6 pad_add_fusion.refs_0_
  42.5 1.3 %reshape.39.refs_2_.refs_5_ = bf16[1,2048]{1,0:T(2,128)(2,1)} reshape(bf16[2048]{0:T(1024)(128)(2,1)} %param.7) | data formatting | bytes 8192 | tf_op jit(solution)/shard_map/reshape | solution.py:213
  43.8 6.5 %shard_map.85 = (bf16[1,4,256,2,512]{4,3,2,1,0:T(2,128)(2,1)}, bf16[4,4,256]{2,1,0:T(4,128)(2,1)}, f32[1,512]{1,0:T(1,128)}, f32[1,512]{1,0:T(1,128)}) custom-call(s32[2]{0:T(128)} %pad_add_fusion.3.refs_0_, bf16[4,256,2048]{2,1,0:T(8,128)(2,1)} %refs_1_.1, bf16[1,2048]{1,0:T(2,128)(2,1)} %reshape.39.refs_2_.refs_5_, bf16[2048,512]{1,0:T(8,128)(2,1)} %refs_6_.5, ...), custom_call_target="tpu_custom_call" | custom-call | tf_op jit(solution)/shard_map/pallas_call | solution.py:170
  50.4 6.8 %shard_map.86 = (bf16[1,4,256,2,512]{4,3,2,1,0:T(2,128)(2,1)}, bf16[4,4,256]{2,1,0:T(4,128)(2,1)}, f32[1,512]{1,0:T(1,128)}, f32[1,512]{1,0:T(1,128)}) custom-call(s32[2]{0:T(128)} %pad_add_fusion.2.refs_0_, bf16[256,512]{1,0:T(8,128)(2,1)} %copy-done.2, bf16[256,512]{1,0:T(8,128)(2,1)} %copy-done.6, ...), custom_call_target="tpu_custom_call", output_to_operand_aliasing={{0}: (10, {}), {1}: (11, {})} | custom-call | tf_op jit(solution)/shard_map/pallas_call | solution.py:170
  57.2 0.0 collective-permute-done.6.refs_2_
  57.3 0.7 copy-done.9
  57.9 0.1 copy-done.11
  58.0 6.8 %shard_map.87 = (bf16[1,4,256,2,512]{4,3,2,1,0:T(2,128)(2,1)}, bf16[4,4,256]{2,1,0:T(4,128)(2,1)}, f32[1,512]{1,0:T(1,128)}, f32[1,512]{1,0:T(1,128)}) custom-call(s32[2]{0:T(128)} %pad_add_fusion.1.refs_0_, bf16[256,512]{1,0:T(8,128)(2,1)} %copy-done.1, bf16[256,512]{1,0:T(8,128)(2,1)} %copy-done.9, ...), custom_call_target="tpu_custom_call", output_to_operand_aliasing={{0}: (10, {}), {1}: (11, {})} | custom-call | tf_op jit(solution)/shard_map/pallas_call | solution.py:170
  64.9 0.0 collective-permute-done.4.refs_8_
  64.9 0.0 collective-permute-done.3.refs_4_
  64.9 0.5 copy-done.14
  65.4 0.2 copy-done.7
  65.6 0.1 copy-done.8
  65.7 6.8 %shard_map.88 = (bf16[1,4,256,2,512]{4,3,2,1,0:T(2,128)(2,1)}, bf16[4,4,256]{2,1,0:T(4,128)(2,1)}, f32[1,512]{1,0:T(1,128)}, f32[1,512]{1,0:T(1,128)}) custom-call(s32[2]{0:T(128)} %pad_add_fusion.refs_0_, bf16[256,512]{1,0:T(8,128)(2,1)} %copy-done, bf16[256,512]{1,0:T(8,128)(2,1)} %copy-done.7, ...), custom_call_target="tpu_custom_call", output_to_operand_aliasing={{0}: (10, {}), {1}: (11, {})} | custom-call | tf_op jit(solution)/shard_map/pallas_call | solution.py:170
  72.6 0.7 multiply_add_fusion
  73.3 1.9 %collective-permute-start.15 = (f32[1,512]{1,0:T(1,128)S(1)}, f32[1,512]{1,0:T(1,128)S(1)}, u32[]{:S(2)}, u32[]{:S(2)}) collective-permute-start(f32[1,512]{1,0:T(1,128)S(1)} %multiply_add_fusion), channel_id=1, source_target_pairs={{0,8},{4,12},{8,0},{12,4},{1,9},{5,13},{9,1},{13,5},{2,10},{6,14},... | collective-permute-start | bytes 6152 | tf_op jit(solution)/shard_map/ppermute | solution.py:196
  75.3 2.7 %collective-permute-start.16 = (f32[1,512]{1,0:T(1,128)S(1)}, f32[1,512]{1,0:T(1,128)S(1)}, u32[]{:S(2)}, u32[]{:S(2)}) collective-permute-start(f32[1,512]{1,0:T(1,128)S(1)} %multiply_add_fusion), channel_id=1, source_target_pairs={{0,12},{4,8},{8,4},{12,0},{1,13},{5,9},{9,5},{13,1},{2,14},{6,10},... | collective-permute-start | bytes 6152 | tf_op jit(solution)/shard_map/ppermute | solution.py:196
  77.9 2.7 %collective-permute-done.16 = f32[1,512]{1,0:T(1,128)S(1)} collective-permute-done((f32[1,512]{1,0:T(1,128)S(1)}, f32[1,512]{1,0:T(1,128)S(1)}, u32[]{:S(2)}, u32[]{:S(2)}) %collective-permute-start.16) | collective-permute-done | bytes 2080 | tf_op jit(solution)/shard_map/ppermute | solution.py:196
  80.6 0.9 %collective-permute-done.17 = f32[1,512]{1,0:T(1,128)S(1)} collective-permute-done((f32[1,512]{1,0:T(1,128)S(1)}, f32[1,512]{1,0:T(1,128)S(1)}, u32[]{:S(2)}, u32[]{:S(2)}) %collective-permute-start.17) | collective-permute-done | bytes 2080 | tf_op jit(solution)/shard_map/ppermute | solution.py:196
  81.5 0.7 select_select_fusion
  (46 shorter events, 0.1 us)
Async XLA Ops:
  1.8 9.8 %collective-permute-start.10 = (bf16[256,512]{1,0:T(8,128)(2,1)S(1)}, bf16[256,512]{1,0:T(8,128)(2,1)S(1)}, u32[]{:S(2)}, u32[]{:S(2)}) collective-permute-start(bf16[256,512]{1,0:T(8,128)(2,1)S(1)} %get-tuple-element.35), channel_id=1, source_target_pairs={{0,4},{4,0},{8,12},{12,8},{1,5},{5,1},{9,13},{13,9},{2,6},{6,2},{1... | collective-permute-start | bytes 786440 | tf_op jit(solution)/shard_map/ppermute | solution.py:196
  5.0 15.3 %collective-permute-start.5 = (bf16[256,512]{1,0:T(8,128)(2,1)S(1)}, bf16[256,512]{1,0:T(8,128)(2,1)S(1)}, u32[]{:S(2)}, u32[]{:S(2)}) collective-permute-start(bf16[256,512]{1,0:T(8,128)(2,1)S(1)} %get-tuple-element.36), channel_id=1, source_target_pairs={{0,12},{4,8},{8,4},{12,0},{1,13},{5,9},{9,5},{13,1},{2,14},{6,10},... | collective-permute-start | bytes 786440 | tf_op jit(solution)/shard_map/ppermute | solution.py:196
  7.4 23.0 %collective-permute-start = (bf16[256,512]{1,0:T(8,128)(2,1)S(1)}, bf16[256,512]{1,0:T(8,128)(2,1)S(1)}, u32[]{:S(2)}, u32[]{:S(2)}) collective-permute-start(bf16[256,512]{1,0:T(8,128)(2,1)S(1)} %get-tuple-element.37), channel_id=1, source_target_pairs={{0,8},{4,12},{8,0},{12,4},{1,9},{5,13},{9,1},{13,5},{2,10},{6,14},... | collective-permute-start | bytes 786440 | tf_op jit(solution)/shard_map/ppermute | solution.py:196
  11.7 38.7 %copy-start.2 = (bf16[256,512]{1,0:T(8,128)(2,1)}, bf16[256,512]{1,0:T(8,128)(2,1)S(1)}, u32[]{:S(2)}) copy-start(bf16[256,512]{1,0:T(8,128)(2,1)S(1)} %collective-permute-done.10.refs_1_) | copy-start | bytes 786436
  11.7 23.5 %collective-permute-start.12 = (bf16[256,512]{1,0:T(8,128)(2,1)S(1)}, bf16[256,512]{1,0:T(8,128)(2,1)S(1)}, u32[]{:S(2)}, u32[]{:S(2)}) collective-permute-start(bf16[256,512]{1,0:T(8,128)(2,1)S(1)} %collective-permute-done.10.refs_1_), channel_id=1, source_target_pairs={{0,2},{1,3},{2,0},{3,1},{4,6},{5,7},{6,4},{7,5},{8,10},{9,11},{10,... | collective-permute-start | bytes 786440 | tf_op jit(solution)/shard_map/ppermute | solution.py:196
  13.9 18.6 %collective-permute-start.14 = (bf16[4,256]{1,0:T(4,128)(2,1)S(1)}, bf16[4,256]{1,0:T(4,128)(2,1)S(1)}, u32[]{:S(2)}, u32[]{:S(2)}) collective-permute-start(bf16[4,256]{1,0:T(4,128)(2,1)S(1)} %get-tuple-element.38), channel_id=1, source_target_pairs={{0,4},{4,0},{8,12},{12,8},{1,5},{5,1},{9,13},{13,9},{2,6},{6,2},{1... | collective-permute-start | bytes 6152 | tf_op jit(solution)/shard_map/ppermute | solution.py:196
  16.3 21.6 %collective-permute-start.11 = (bf16[256,512]{1,0:T(8,128)(2,1)S(1)}, bf16[256,512]{1,0:T(8,128)(2,1)S(1)}, u32[]{:S(2)}, u32[]{:S(2)}) collective-permute-start(bf16[256,512]{1,0:T(8,128)(2,1)S(1)} %collective-permute-done.10.refs_1_), channel_id=1, source_target_pairs={{0,1},{1,0},{2,3},{3,2},{4,5},{5,4},{6,7},{7,6},{8,9},{9,8},{10,11... | collective-permute-start | bytes 786440 | tf_op jit(solution)/shard_map/ppermute | solution.py:196
  20.3 30.0 %copy-start.1 = (bf16[256,512]{1,0:T(8,128)(2,1)}, bf16[256,512]{1,0:T(8,128)(2,1)S(1)}, u32[]{:S(2)}) copy-start(bf16[256,512]{1,0:T(8,128)(2,1)S(1)} %collective-permute-done.5.refs_1_) | copy-start | bytes 786436
  20.3 18.1 %collective-permute-start.7 = (bf16[256,512]{1,0:T(8,128)(2,1)S(1)}, bf16[256,512]{1,0:T(8,128)(2,1)S(1)}, u32[]{:S(2)}, u32[]{:S(2)}) collective-permute-start(bf16[256,512]{1,0:T(8,128)(2,1)S(1)} %collective-permute-done.5.refs_1_), channel_id=1, source_target_pairs={{0,2},{1,3},{2,0},{3,1},{4,6},{5,7},{6,4},{7,5},{8,10},{9,11},{10,... | collective-permute-start | bytes 786440 | tf_op jit(solution)/shard_map/ppermute | solution.py:196
  30.4 19.9 %copy-start = (bf16[256,512]{1,0:T(8,128)(2,1)}, bf16[256,512]{1,0:T(8,128)(2,1)S(1)}, u32[]{:S(2)}) copy-start(bf16[256,512]{1,0:T(8,128)(2,1)S(1)} %collective-permute-done.refs_1_) | copy-start | bytes 786436
  30.4 8.1 %collective-permute-start.2 = (bf16[256,512]{1,0:T(8,128)(2,1)S(1)}, bf16[256,512]{1,0:T(8,128)(2,1)S(1)}, u32[]{:S(2)}, u32[]{:S(2)}) collective-permute-start(bf16[256,512]{1,0:T(8,128)(2,1)S(1)} %collective-permute-done.refs_1_), channel_id=1, source_target_pairs={{0,2},{1,3},{2,0},{3,1},{4,6},{5,7},{6,4},{7,5},{8,10},{9,11},{10,... | collective-permute-start | bytes 786440 | tf_op jit(solution)/shard_map/ppermute | solution.py:196
  32.5 17.8 %copy-start.12 = (bf16[4,256]{1,0:T(4,128)(2,1)}, bf16[4,256]{1,0:T(4,128)(2,1)S(1)}, u32[]{:S(2)}) copy-start(bf16[4,256]{1,0:T(4,128)(2,1)S(1)} %collective-permute-done.14.refs_8_) | copy-start | bytes 6148
  32.5 5.4 %collective-permute-start.9 = (bf16[4,256]{1,0:T(4,128)(2,1)S(1)}, bf16[4,256]{1,0:T(4,128)(2,1)S(1)}, u32[]{:S(2)}, u32[]{:S(2)}) collective-permute-start(bf16[4,256]{1,0:T(4,128)(2,1)S(1)} %get-tuple-element.39), channel_id=1, source_target_pairs={{0,12},{4,8},{8,4},{12,0},{1,13},{5,9},{9,5},{13,1},{2,14},{6,10},... | collective-permute-start | bytes 6152 | tf_op jit(solution)/shard_map/ppermute | solution.py:196
  35.1 15.2 %copy-start.4 = (bf16[256,512]{1,0:T(8,128)(2,1)}, bf16[256,512]{1,0:T(8,128)(2,1)S(1)}, u32[]{:S(2)}) copy-start(bf16[256,512]{1,0:T(8,128)(2,1)S(1)} %collective-permute-done.12.refs_3_) | copy-start | bytes 786436
  35.2 5.6 %collective-permute-start.13 = (bf16[256,512]{1,0:T(8,128)(2,1)S(1)}, bf16[256,512]{1,0:T(8,128)(2,1)S(1)}, u32[]{:S(2)}, u32[]{:S(2)}) collective-permute-start(bf16[256,512]{1,0:T(8,128)(2,1)S(1)} %collective-permute-done.12.refs_3_), channel_id=1, source_target_pairs={{0,1},{1,0},{2,3},{3,2},{4,5},{5,4},{6,7},{7,6},{8,9},{9,8},{10,11... | collective-permute-start | bytes 786440 | tf_op jit(solution)/shard_map/ppermute | solution.py:196
  37.9 12.5 %copy-start.13 = (bf16[4,256]{1,0:T(4,128)(2,1)}, bf16[4,256]{1,0:T(4,128)(2,1)S(1)}, u32[]{:S(2)}) copy-start(bf16[4,256]{1,0:T(4,128)(2,1)S(1)} %collective-permute-done.9.refs_8_) | copy-start | bytes 6148
  37.9 19.3 %collective-permute-start.6 = (bf16[256,512]{1,0:T(8,128)(2,1)S(1)}, bf16[256,512]{1,0:T(8,128)(2,1)S(1)}, u32[]{:S(2)}, u32[]{:S(2)}) collective-permute-start(bf16[256,512]{1,0:T(8,128)(2,1)S(1)} %collective-permute-done.5.refs_1_), channel_id=1, source_target_pairs={{0,1},{1,0},{2,3},{3,2},{4,5},{5,4},{6,7},{7,6},{8,9},{9,8},{10,11... | collective-permute-start | bytes 786440 | tf_op jit(solution)/shard_map/ppermute | solution.py:196
  37.9 12.5 %copy-start.6 = (bf16[256,512]{1,0:T(8,128)(2,1)}, bf16[256,512]{1,0:T(8,128)(2,1)S(1)}, u32[]{:S(2)}) copy-start(bf16[256,512]{1,0:T(8,128)(2,1)S(1)} %collective-permute-done.11.refs_2_) | copy-start | bytes 786436
  37.9 27.0 %collective-permute-start.1 = (bf16[256,512]{1,0:T(8,128)(2,1)S(1)}, bf16[256,512]{1,0:T(8,128)(2,1)S(1)}, u32[]{:S(2)}, u32[]{:S(2)}) collective-permute-start(bf16[256,512]{1,0:T(8,128)(2,1)S(1)} %collective-permute-done.refs_1_), channel_id=1, source_target_pairs={{0,1},{1,0},{2,3},{3,2},{4,5},{5,4},{6,7},{7,6},{8,9},{9,8},{10,11... | collective-permute-start | bytes 786440 | tf_op jit(solution)/shard_map/ppermute | solution.py:196
  38.4 12.0 %copy-start.5 = (bf16[256,512]{1,0:T(8,128)(2,1)}, bf16[256,512]{1,0:T(8,128)(2,1)S(1)}, u32[]{:S(2)}) copy-start(bf16[256,512]{1,0:T(8,128)(2,1)S(1)} %collective-permute-done.7.refs_3_) | copy-start | bytes 786436
  38.4 18.8 %collective-permute-start.8 = (bf16[256,512]{1,0:T(8,128)(2,1)S(1)}, bf16[256,512]{1,0:T(8,128)(2,1)S(1)}, u32[]{:S(2)}, u32[]{:S(2)}) collective-permute-start(bf16[256,512]{1,0:T(8,128)(2,1)S(1)} %collective-permute-done.7.refs_3_), channel_id=1, source_target_pairs={{0,1},{1,0},{2,3},{3,2},{4,5},{5,4},{6,7},{7,6},{8,9},{9,8},{10,11... | collective-permute-start | bytes 786440 | tf_op jit(solution)/shard_map/ppermute | solution.py:196
  38.5 11.9 %copy-start.3 = (bf16[256,512]{1,0:T(8,128)(2,1)}, bf16[256,512]{1,0:T(8,128)(2,1)S(1)}, u32[]{:S(2)}) copy-start(bf16[256,512]{1,0:T(8,128)(2,1)S(1)} %collective-permute-done.2.refs_3_) | copy-start | bytes 786436
  38.5 26.4 %collective-permute-start.3 = (bf16[256,512]{1,0:T(8,128)(2,1)S(1)}, bf16[256,512]{1,0:T(8,128)(2,1)S(1)}, u32[]{:S(2)}, u32[]{:S(2)}) collective-permute-start(bf16[256,512]{1,0:T(8,128)(2,1)S(1)} %collective-permute-done.2.refs_3_), channel_id=1, source_target_pairs={{0,1},{1,0},{2,3},{3,2},{4,5},{5,4},{6,7},{7,6},{8,9},{9,8},{10,11... | collective-permute-start | bytes 786440 | tf_op jit(solution)/shard_map/ppermute | solution.py:196
  40.8 9.6 %copy-start.10 = (bf16[256,512]{1,0:T(8,128)(2,1)}, bf16[256,512]{1,0:T(8,128)(2,1)S(1)}, u32[]{:S(2)}) copy-start(bf16[256,512]{1,0:T(8,128)(2,1)S(1)} %collective-permute-done.13.refs_4_) | copy-start | bytes 786436
  40.8 24.1 %collective-permute-start.4 = (bf16[4,256]{1,0:T(4,128)(2,1)S(1)}, bf16[4,256]{1,0:T(4,128)(2,1)S(1)}, u32[]{:S(2)}, u32[]{:S(2)}) collective-permute-start(bf16[4,256]{1,0:T(4,128)(2,1)S(1)} %get-tuple-element.40), channel_id=1, source_target_pairs={{0,8},{4,12},{8,0},{12,4},{1,9},{5,13},{9,1},{13,5},{2,10},{6,14},... | collective-permute-start | bytes 6152 | tf_op jit(solution)/shard_map/ppermute | solution.py:196
  57.2 0.7 copy-start.9
  57.2 0.8 copy-start.11
  64.9 0.6 copy-start.14
  64.9 0.7 copy-start.7
  64.9 0.8 copy-start.8
  65.7 6.9 %copy-start.15 = (f32[1,512]{1,0:T(1,128)S(1)}, f32[1,512]{1,0:T(1,128)}, u32[]{:S(2)}) copy-start(f32[1,512]{1,0:T(1,128)} %get-tuple-element.27) | copy-start | bytes 6148
  65.7 6.9 %copy-start.16 = (f32[1,512]{1,0:T(1,128)S(1)}, f32[1,512]{1,0:T(1,128)}, u32[]{:S(2)}) copy-start(f32[1,512]{1,0:T(1,128)} %get-tuple-element.32) | copy-start | bytes 6148
  65.7 6.9 %copy-start.17 = (f32[1,512]{1,0:T(1,128)S(1)}, f32[1,512]{1,0:T(1,128)}, u32[]{:S(2)}) copy-start(f32[1,512]{1,0:T(1,128)} %get-tuple-element.31) | copy-start | bytes 6148
  65.7 6.9 %copy-start.18 = (f32[1,512]{1,0:T(1,128)S(1)}, f32[1,512]{1,0:T(1,128)}, u32[]{:S(2)}) copy-start(f32[1,512]{1,0:T(1,128)} %get-tuple-element.28) | copy-start | bytes 6148
  65.7 6.9 %copy-start.19 = (f32[1,512]{1,0:T(1,128)S(1)}, f32[1,512]{1,0:T(1,128)}, u32[]{:S(2)}) copy-start(f32[1,512]{1,0:T(1,128)} %get-tuple-element.33) | copy-start | bytes 6148
  65.7 6.9 %copy-start.20 = (f32[1,512]{1,0:T(1,128)S(1)}, f32[1,512]{1,0:T(1,128)}, u32[]{:S(2)}) copy-start(f32[1,512]{1,0:T(1,128)} %get-tuple-element.29) | copy-start | bytes 6148
  73.3 4.6 %collective-permute-start.15 = (f32[1,512]{1,0:T(1,128)S(1)}, f32[1,512]{1,0:T(1,128)S(1)}, u32[]{:S(2)}, u32[]{:S(2)}) collective-permute-start(f32[1,512]{1,0:T(1,128)S(1)} %multiply_add_fusion), channel_id=1, source_target_pairs={{0,8},{4,12},{8,0},{12,4},{1,9},{5,13},{9,1},{13,5},{2,10},{6,14},... | collective-permute-start | bytes 6152 | tf_op jit(solution)/shard_map/ppermute | solution.py:196
  75.3 5.4 %collective-permute-start.16 = (f32[1,512]{1,0:T(1,128)S(1)}, f32[1,512]{1,0:T(1,128)S(1)}, u32[]{:S(2)}, u32[]{:S(2)}) collective-permute-start(f32[1,512]{1,0:T(1,128)S(1)} %multiply_add_fusion), channel_id=1, source_target_pairs={{0,12},{4,8},{8,4},{12,0},{1,13},{5,9},{9,5},{13,1},{2,14},{6,10},... | collective-permute-start | bytes 6152 | tf_op jit(solution)/shard_map/ppermute | solution.py:196
  77.9 3.6 %collective-permute-start.17 = (f32[1,512]{1,0:T(1,128)S(1)}, f32[1,512]{1,0:T(1,128)S(1)}, u32[]{:S(2)}, u32[]{:S(2)}) collective-permute-start(f32[1,512]{1,0:T(1,128)S(1)} %multiply_add_fusion), channel_id=1, source_target_pairs={{0,4},{4,0},{8,12},{12,8},{1,5},{5,1},{9,13},{13,9},{2,6},{6,2},{1... | collective-permute-start | bytes 6152 | tf_op jit(solution)/shard_map/ppermute | solution.py:196

commit v2 on v1

--- a/solution.py
+++ b/solution.py
@@ -84,7 +84,12 @@
     parts = refs[1 : 1 + part_count]
     gain_ref, key_ref, value_ref, bias_ref, query_ref = refs[1 + part_count : 6 + part_count]
     rest = refs[6 + part_count + (2 if carried else 0) :]
-    cache_ref, bias_out_ref, partial_ref, total_ref, normed_ref = rest
+    cache_ref, bias_out_ref, partial_ref, total_ref = rest[:4]
+    normed_ref, key_local, value_local, weight_sems = rest[4:]
+    key_copy = pltpu.make_async_copy(key_ref, key_local, weight_sems.at[0])
+    value_copy = pltpu.make_async_copy(value_ref, value_local, weight_sems.at[1])
+    key_copy.start()
+    value_copy.start()
     piece, width = normed_ref.shape
     heads_here = bias_ref.shape[-2]
     columns = key_ref.shape[1]
@@ -108,10 +113,12 @@
             scaled = part[...].astype(jnp.float32) * inverse * own_gain
             normed_ref[:, pl.ds(start, share)] = scaled.astype(jnp.bfloat16)
     normed = normed_ref[...]
-    key_rows = jnp.dot(normed, key_ref[...], preferred_element_type=jnp.float32).astype(
+    key_copy.wait()
+    key_rows = jnp.dot(normed, key_local[...], preferred_element_type=jnp.float32).astype(
         jnp.bfloat16
     )
-    value_rows = jnp.dot(normed, value_ref[...], preferred_element_type=jnp.float32).astype(
+    value_copy.wait()
+    value_rows = jnp.dot(normed, value_local[...], preferred_element_type=jnp.float32).astype(
         jnp.bfloat16
     )
     cache_ref[0, 0] = jnp.stack((key_rows, value_rows), axis=1)
@@ -160,12 +167,13 @@
         part_specs = [full(part) for part in parts]
         bias_spec = full(bias)
     operands = [index, *parts, gain, key_weight, value_weight, bias, query]
-    specs = part_specs + [full(gain), full(key_weight), full(value_weight), bias_spec, full(query)]
+    in_place = pl.BlockSpec(memory_space=pl.ANY)
+    specs = part_specs + [full(gain), in_place, in_place, bias_spec, full(query)]
     aliases = {}
     if carried is not None:
         aliases = {len(operands): 0, len(operands) + 1: 1}
         operands += list(carried)
-        specs += [pl.BlockSpec(memory_space=pl.ANY)] * 2
+        specs += [in_place] * 2
     row = jax.ShapeDtypeStruct((1, columns), jnp.float32)
     return pl.pallas_call(
         functools.partial(block_kernel, part_count, whole_rows, carried is not None),
@@ -179,7 +187,12 @@
                 pl.BlockSpec((1, columns), lambda g, s: (0, 0)),
                 pl.BlockSpec((1, columns), lambda g, s: (0, 0)),
             ],
-            scratch_shapes=[pltpu.VMEM((piece, width), jnp.bfloat16)],
+            scratch_shapes=[
+                pltpu.VMEM((piece, width), jnp.bfloat16),
+                pltpu.VMEM((width, columns), jnp.bfloat16),
+                pltpu.VMEM((width, columns), jnp.bfloat16),
+                pltpu.SemaphoreType.DMA((2,)),
+            ],
         ),
         out_shape=[
             jax.ShapeDtypeStruct((1, block_count, piece, 2, columns), jnp.bfloat16),
@@ -188,12 +201,21 @@
             row,
         ],
         input_output_aliases=aliases,
+        cost_estimate=pl.CostEstimate(
+            flops=4 * piece * width * columns,
+            transcendentals=3 * heads_here * piece,
+            bytes_accessed=4 * width * columns + 2 * piece * (width + 2 * columns),
+        ),
     )(*operands)
 
 
 def swap(array, axis, offset):
     size = lax.axis_size(axis)
     return lax.ppermute(array, axis, [(k, k ^ offset) for k in range(size)])
+
+
+def after(array, block):
+    return lax.optimization_barrier((array, block[3]))[0]
 
 
 def exchange_order(size):
@@ -208,7 +230,6 @@
     own = lax.axis_index("sp")
     own_share = lax.axis_index("tp")
     bias_rows = jnp.transpose(break_bias, (0, 2, 1))
-    heads_here = bias_rows.shape[1]
     columns = key_weight.shape[1]
     gain = norm_gain.reshape(1, width)
     query = lax.dynamic_slice_in_dim(new_query, own, 1, 0).astype(jnp.float32)
@@ -229,15 +250,28 @@
         bias_arrived[offset] = swap(bias_sent, "sp", offset)
     built = {}
     built[0] = build_block(
-        index_of(0), [tokens], gain, key_weight, value_weight, bias_rows, query, None, block_count
+        index_of(0),
+        [tokens],
+        gain,
+        key_weight,
+        value_weight,
+        bias_rows,
+        query,
+        None,
+        block_count,
     )
     latest = built[0]
-    for offset in order:
+    for place, offset in enumerate(order):
         shares = {0: arrived[offset]}
+        if place != 1:
+            shares[0] = after(shares[0], built[order[place - 2] if place else 0])
         bit = share_count // 2
         while bit:
             for known in list(shares):
-                shares[known | bit] = swap(shares[known], "tp", bit)
+                sent = shares[known]
+                if known and place > 1:
+                    sent = after(sent, latest)
+                shares[known | bit] = swap(sent, "tp", bit)
             bit //= 2
         parts = [shares[k] for k in range(share_count)]
         latest = build_block(

time: 82.5 us -> 77.3 us (0.937)
  waiting for transfers between devices: 22.4 us -> 18.1 us
  starting transfers between devices: 22 us -> 21.1 us
    ppermute x18, waiting for transfers between devices: 22.4 us -> 18.1 us  [swap(): return lax.ppermute(array, axis, [(k, k ^ offset) for k in range(size)])]
    ppermute x18, starting transfers between devices: 22 us -> 21.1 us  [swap(): return lax.ppermute(array, axis, [(k, k ^ offset) for k in range(size)])]
    unnamed x42 -> x44, local copies, waits for them, and re-layouts: 1.65 us -> 2.43 us
  transfers between devices with their start and end apart: 18 -> 18, of which waited for: 6 -> 8; matrix products, arithmetic and copies ran while one was open for 7% -> 6% of each run, Pallas kernels for 25% -> 26%
where the time goes in v2:
time: 77.3 us; the launch traced here: 76.9 us
  Pallas kernels  26.9 us (35%)
  starting transfers between devices  21.1 us (27%)
  waiting for transfers between devices  18.1 us (23%)
  other arithmetic  5.02 us (6%)
  local copies, waits for them, and re-layouts  4.9 us (6%)
  between operations  0.92 us (1%)
    pallas_call x4, Pallas kernels, build_block(): pl.pallas_call(functools.partial(block_kernel, part_count, whole_rows, ca...  26.9 us
    ppermute x18, starting transfers between devices, swap(): return lax.ppermute(array, axis, [(k, k ^ offset) for k in range(size)])  21.1 us
    ppermute x18, waiting for transfers between devices, swap(): return lax.ppermute(array, axis, [(k, k ^ offset) for k in range(size)])  18.1 us
    unnamed x44, local copies, waits for them, and re-layouts  2.43 us
    another operation x4, other arithmetic, index_of(): return jnp.stack((own ^ offset, own_share)).astype(jnp.int32)  2.33 us
  transfers between devices with their start and end apart: 18, of which 8 were waited for; matrix products, arithmetic and copies ran while one was open for 6% of the time, Pallas kernels for 26%

profile of v2, /device:TPU:0, one launch (start us, length us, event | category | flops | bytes accessed | tf_op | source)
XLA Modules:
  0.0 76.9 jit_solution(16039332803221592459)
XLA Ops:
  0.7 1.2 %dynamic-slice_bitcast_fusion = (bf16[256,512]{1,0:T(8,128)(2,1)S(1)}, bf16[256,512]{1,0:T(8,128)(2,1)S(1)}, bf16[256,512]{1,0:T(8,128)(2,1)S(1)}) fusion(bf16[4,256,2048]{2,1,0:T(8,128)(2,1)} %refs_1_.1, s32[]{:T(128)S(6)} %select_n.113, s32[]{:T(128)S(6)} %select_n.110, s32[]{:T(128)S(6)} %select_n.111, s32[]{:T(128)S(6)} %select_n.109), kind=kLoop, calls=%fused_computation | loop fusion | bytes 1572880 | tf_op jit(solution)/shard_map/reshape | solution.py:246
  1.8 3.1 %collective-permute-start.1 = (bf16[256,512]{1,0:T(8,128)(2,1)S(1)}, bf16[256,512]{1,0:T(8,128)(2,1)S(1)}, u32[]{:S(2)}, u32[]{:S(2)}) collective-permute-start(bf16[256,512]{1,0:T(8,128)(2,1)S(1)} %get-tuple-element.42), channel_id=1, source_target_pairs={{0,4},{4,0},{8,12},{12,8},{1,5},{5,1},{9,13},{13,9},{2,6},{6,2},{1... | collective-permute-start | bytes 786440 | tf_op jit(solution)/shard_map/ppermute | solution.py:214
  5.0 2.5 %collective-permute-start.8 = (bf16[256,512]{1,0:T(8,128)(2,1)S(1)}, bf16[256,512]{1,0:T(8,128)(2,1)S(1)}, u32[]{:S(2)}, u32[]{:S(2)}) collective-permute-start(bf16[256,512]{1,0:T(8,128)(2,1)S(1)} %get-tuple-element.41), channel_id=1, source_target_pairs={{0,12},{4,8},{8,4},{12,0},{1,13},{5,9},{9,5},{13,1},{2,14},{6,10},... | collective-permute-start | bytes 786440 | tf_op jit(solution)/shard_map/ppermute | solution.py:214
  7.4 0.6 pad_add_fusion.2.refs_0_
  8.0 1.3 %reshape.40.refs_2_.refs_5_ = bf16[1,2048]{1,0:T(2,128)(2,1)} reshape(bf16[2048]{0:T(1024)(128)(2,1)} %param.7) | data formatting | bytes 8192 | tf_op jit(solution)/shard_map/reshape | solution.py:234
  9.3 1.3 %dynamic-slice_convert_fusion.refs_6_.refs_9_ = f32[1,512]{1,0:T(1,128)} fusion(bf16[4,512]{1,0:T(4,128)(2,1)} %param.11, s32[]{:T(128)S(6)} %select_n.112), kind=kLoop, calls=%fused_computation.28 | loop fusion | flops 512 | bytes 3076 | tf_op jit(solution)/shard_map/convert_element_type | solution.py:235
  10.6 6.9 %shard_map.85 = (bf16[1,4,256,2,512]{4,3,2,1,0:T(2,128)(2,1)}, bf16[4,4,256]{2,1,0:T(4,128)(2,1)}, f32[1,512]{1,0:T(1,128)}, f32[1,512]{1,0:T(1,128)}) custom-call(s32[2]{0:T(128)} %pad_add_fusion.2.refs_0_, bf16[4,256,2048]{2,1,0:T(8,128)(2,1)} %refs_1_.1, bf16[1,2048]{1,0:T(2,128)(2,1)} %reshape.40.refs_2_.refs_5_, bf16[2048,512]{1,0:T(8,128)(2,1)} %refs_6_.5, ...), custom_call_target="tpu_custom_call" | custom-call | flops 1073741824 | bytes 5767168 | tf_op jit(solution)/shard_map/pallas_call | solution.py:178
  17.5 1.6 %collective-permute-start.3 = (bf16[256,512]{1,0:T(8,128)(2,1)S(1)}, bf16[256,512]{1,0:T(8,128)(2,1)S(1)}, u32[]{:S(2)}, u32[]{:S(2)}) collective-permute-start(bf16[256,512]{1,0:T(8,128)(2,1)S(1)} %collective-permute-done.1.refs_1_), channel_id=1, source_target_pairs={{0,2},{1,3},{2,0},{3,1},{4,6},{5,7},{6,4},{7,5},{8,10},{9,11},{10,... | collective-permute-start | bytes 786440 | tf_op jit(solution)/shard_map/ppermute | solution.py:214
  19.0 0.1 collective-permute-done.8.refs_1_
  19.2 1.5 %collective-permute-start.10 = (bf16[256,512]{1,0:T(8,128)(2,1)S(1)}, bf16[256,512]{1,0:T(8,128)(2,1)S(1)}, u32[]{:S(2)}, u32[]{:S(2)}) collective-permute-start(bf16[256,512]{1,0:T(8,128)(2,1)S(1)} %collective-permute-done.8.refs_1_), channel_id=1, source_target_pairs={{0,2},{1,3},{2,0},{3,1},{4,6},{5,7},{6,4},{7,5},{8,10},{9,11},{10,... | collective-permute-start | bytes 786440 | tf_op jit(solution)/shard_map/ppermute | solution.py:214
  20.7 0.0 collective-permute-start.2
  20.7 6.1 %collective-permute-done.3.refs_3_ = bf16[256,512]{1,0:T(8,128)(2,1)S(1)} collective-permute-done((bf16[256,512]{1,0:T(8,128)(2,1)S(1)}, bf16[256,512]{1,0:T(8,128)(2,1)S(1)}, u32[]{:S(2)}, u32[]{:S(2)}) %collective-permute-start.3) | collective-permute-done | bytes 262176 | tf_op jit(solution)/shard_map/ppermute | solution.py:214
  26.7 0.0 collective-permute-start.4
  26.7 0.1 collective-permute-start
  26.8 3.0 %collective-permute-start.5 = (bf16[4,256]{1,0:T(4,128)(2,1)S(1)}, bf16[4,256]{1,0:T(4,128)(2,1)S(1)}, u32[]{:S(2)}, u32[]{:S(2)}) collective-permute-start(bf16[4,256]{1,0:T(4,128)(2,1)S(1)} %get-tuple-element.45), channel_id=1, source_target_pairs={{0,4},{4,0},{8,12},{12,8},{1,5},{5,1},{9,13},{13,9},{2,6},{6,2},{1... | collective-permute-start | bytes 6152 | tf_op jit(solution)/shard_map/ppermute | solution.py:214
  29.8 0.6 pad_add_fusion.1.refs_0_
  30.4 2.9 %collective-permute-done.5.refs_8_ = bf16[4,256]{1,0:T(4,128)(2,1)S(1)} collective-permute-done((bf16[4,256]{1,0:T(4,128)(2,1)S(1)}, bf16[4,256]{1,0:T(4,128)(2,1)S(1)}, u32[]{:S(2)}, u32[]{:S(2)}) %collective-permute-start.5) | collective-permute-done | bytes 2080 | tf_op jit(solution)/shard_map/ppermute | solution.py:214
  33.3 0.5 collective-permute-start.11
  33.9 0.0 collective-permute-done.4.refs_4_
  33.9 0.0 copy-done.14
  33.9 0.6 copy-done.8
  34.6 0.1 copy-done.10
  34.7 6.7 %shard_map.86 = (bf16[1,4,256,2,512]{4,3,2,1,0:T(2,128)(2,1)}, bf16[4,4,256]{2,1,0:T(4,128)(2,1)}, f32[1,512]{1,0:T(1,128)}, f32[1,512]{1,0:T(1,128)}) custom-call(s32[2]{0:T(128)} %pad_add_fusion.1.refs_0_, bf16[256,512]{1,0:T(8,128)(2,1)} %copy-done.3, bf16[256,512]{1,0:T(8,128)(2,1)} %copy-done.8, ...), custom_call_target="tpu_custom_call", output_to_operand_aliasing={{0}: (10, {}), {1}: (11, {})} | custom-call | flops 1073741824 | bytes 5767168 | tf_op jit(solution)/shard_map/pallas_call | solution.py:178
  41.3 0.6 collective-permute-done.refs_1_
  42.0 1.5 %collective-permute-start.7 = (bf16[256,512]{1,0:T(8,128)(2,1)S(1)}, bf16[256,512]{1,0:T(8,128)(2,1)S(1)}, u32[]{:S(2)}, u32[]{:S(2)}) collective-permute-start(bf16[256,512]{1,0:T(8,128)(2,1)S(1)} %collective-permute-done.refs_1_), channel_id=1, source_target_pairs={{0,2},{1,3},{2,0},{3,1},{4,6},{5,7},{6,4},{7,5},{8,10},{9,11},{10,... | collective-permute-start | bytes 786440 | tf_op jit(solution)/shard_map/ppermute | solution.py:214
  43.4 2.2 %collective-permute-start.12 = (bf16[4,256]{1,0:T(4,128)(2,1)S(1)}, bf16[4,256]{1,0:T(4,128)(2,1)S(1)}, u32[]{:S(2)}, u32[]{:S(2)}) collective-permute-start(bf16[4,256]{1,0:T(4,128)(2,1)S(1)} %get-tuple-element.46), channel_id=1, source_target_pairs={{0,12},{4,8},{8,4},{12,0},{1,13},{5,9},{9,5},{13,1},{2,14},{6,10},... | collective-permute-start | bytes 6152 | tf_op jit(solution)/shard_map/ppermute | solution.py:214
  45.7 0.6 pad_add_fusion.3.refs_0_
  46.3 0.0 collective-permute-start.6
  46.3 2.6 %collective-permute-done.12.refs_8_ = bf16[4,256]{1,0:T(4,128)(2,1)S(1)} collective-permute-done((bf16[4,256]{1,0:T(4,128)(2,1)S(1)}, bf16[4,256]{1,0:T(4,128)(2,1)S(1)}, u32[]{:S(2)}, u32[]{:S(2)}) %collective-permute-start.12) | collective-permute-done | bytes 2080 | tf_op jit(solution)/shard_map/ppermute | solution.py:214
  48.9 0.6 copy-done.15
  49.4 0.1 copy-done.7
  49.5 0.1 copy-done.9
  49.6 6.7 %shard_map.87 = (bf16[1,4,256,2,512]{4,3,2,1,0:T(2,128)(2,1)}, bf16[4,4,256]{2,1,0:T(4,128)(2,1)}, f32[1,512]{1,0:T(1,128)}, f32[1,512]{1,0:T(1,128)}) custom-call(s32[2]{0:T(128)} %pad_add_fusion.3.refs_0_, bf16[256,512]{1,0:T(8,128)(2,1)} %copy-done.1, bf16[256,512]{1,0:T(8,128)(2,1)} %copy-done.7, ...), custom_call_target="tpu_custom_call", output_to_operand_aliasing={{0}: (10, {}), {1}: (11, {})} | custom-call | flops 1073741824 | bytes 5767168 | tf_op jit(solution)/shard_map/pallas_call | solution.py:178
  56.4 0.1 collective-permute-start.13
  56.4 1.5 %collective-permute-start.14 = (bf16[4,256]{1,0:T(4,128)(2,1)S(1)}, bf16[4,256]{1,0:T(4,128)(2,1)S(1)}, u32[]{:S(2)}, u32[]{:S(2)}) collective-permute-start(bf16[4,256]{1,0:T(4,128)(2,1)S(1)} %get-tuple-element.44), channel_id=1, source_target_pairs={{0,8},{4,12},{8,0},{12,4},{1,9},{5,13},{9,1},{13,5},{2,10},{6,14},... | collective-permute-start | bytes 6152 | tf_op jit(solution)/shard_map/ppermute | solution.py:214
  58.0 0.6 pad_add_fusion.refs_0_
  58.5 2.5 %collective-permute-done.14.refs_8_ = bf16[4,256]{1,0:T(4,128)(2,1)S(1)} collective-permute-done((bf16[4,256]{1,0:T(4,128)(2,1)S(1)}, bf16[4,256]{1,0:T(4,128)(2,1)S(1)}, u32[]{:S(2)}, u32[]{:S(2)}) %collective-permute-start.14) | collective-permute-done | bytes 2080 | tf_op jit(solution)/shard_map/ppermute | solution.py:214
  61.0 0.5 copy-done.13
  61.6 0.1 copy-done.5
  61.7 0.1 copy-done.11
  61.9 6.7 %shard_map.88 = (bf16[1,4,256,2,512]{4,3,2,1,0:T(2,128)(2,1)}, bf16[4,4,256]{2,1,0:T(4,128)(2,1)}, f32[1,512]{1,0:T(1,128)}, f32[1,512]{1,0:T(1,128)}) custom-call(s32[2]{0:T(128)} %pad_add_fusion.refs_0_, bf16[256,512]{1,0:T(8,128)(2,1)} %copy-done, bf16[256,512]{1,0:T(8,128)(2,1)} %copy-done.5, ...), custom_call_target="tpu_custom_call", output_to_operand_aliasing={{0}: (10, {}), {1}: (11, {})} | custom-call | flops 1073741824 | bytes 5767168 | tf_op jit(solution)/shard_map/pallas_call | solution.py:178
  68.6 0.7 multiply_add_fusion
  69.3 1.5 %collective-permute-start.15 = (f32[1,512]{1,0:T(1,128)S(1)}, f32[1,512]{1,0:T(1,128)S(1)}, u32[]{:S(2)}, u32[]{:S(2)}) collective-permute-start(f32[1,512]{1,0:T(1,128)S(1)} %multiply_add_fusion), channel_id=1, source_target_pairs={{0,8},{4,12},{8,0},{12,4},{1,9},{5,13},{9,1},{13,5},{2,10},{6,14},... | collective-permute-start | bytes 6152 | tf_op jit(solution)/shard_map/ppermute | solution.py:214
  70.9 1.1 %collective-permute-start.16 = (f32[1,512]{1,0:T(1,128)S(1)}, f32[1,512]{1,0:T(1,128)S(1)}, u32[]{:S(2)}, u32[]{:S(2)}) collective-permute-start(f32[1,512]{1,0:T(1,128)S(1)} %multiply_add_fusion), channel_id=1, source_target_pairs={{0,12},{4,8},{8,4},{12,0},{1,13},{5,9},{9,5},{13,1},{2,14},{6,10},... | collective-permute-start | bytes 6152 | tf_op jit(solution)/shard_map/ppermute | solution.py:214
  71.9 1.0 %collective-permute-start.17 = (f32[1,512]{1,0:T(1,128)S(1)}, f32[1,512]{1,0:T(1,128)S(1)}, u32[]{:S(2)}, u32[]{:S(2)}) collective-permute-start(f32[1,512]{1,0:T(1,128)S(1)} %multiply_add_fusion), channel_id=1, source_target_pairs={{0,4},{4,0},{8,12},{12,8},{1,5},{5,1},{9,13},{13,9},{2,6},{6,2},{1... | collective-permute-start | bytes 6152 | tf_op jit(solution)/shard_map/ppermute | solution.py:214
  72.9 1.0 %collective-permute-done.15 = f32[1,512]{1,0:T(1,128)S(1)} collective-permute-done((f32[1,512]{1,0:T(1,128)S(1)}, f32[1,512]{1,0:T(1,128)S(1)}, u32[]{:S(2)}, u32[]{:S(2)}) %collective-permute-start.15) | collective-permute-done | bytes 2080 | tf_op jit(solution)/shard_map/ppermute | solution.py:214
  73.9 2.4 %collective-permute-done.16 = f32[1,512]{1,0:T(1,128)S(1)} collective-permute-done((f32[1,512]{1,0:T(1,128)S(1)}, f32[1,512]{1,0:T(1,128)S(1)}, u32[]{:S(2)}, u32[]{:S(2)}) %collective-permute-start.16) | collective-permute-done | bytes 2080 | tf_op jit(solution)/shard_map/ppermute | solution.py:214
  76.2 0.7 select_select_fusion
  (48 shorter events, 0.1 us)
Async XLA Ops:
  1.8 15.6 %collective-permute-start.1 = (bf16[256,512]{1,0:T(8,128)(2,1)S(1)}, bf16[256,512]{1,0:T(8,128)(2,1)S(1)}, u32[]{:S(2)}, u32[]{:S(2)}) collective-permute-start(bf16[256,512]{1,0:T(8,128)(2,1)S(1)} %get-tuple-element.42), channel_id=1, source_target_pairs={{0,4},{4,0},{8,12},{12,8},{1,5},{5,1},{9,13},{13,9},{2,6},{6,2},{1... | collective-permute-start | bytes 786440 | tf_op jit(solution)/shard_map/ppermute | solution.py:214
  5.0 14.2 %collective-permute-start.8 = (bf16[256,512]{1,0:T(8,128)(2,1)S(1)}, bf16[256,512]{1,0:T(8,128)(2,1)S(1)}, u32[]{:S(2)}, u32[]{:S(2)}) collective-permute-start(bf16[256,512]{1,0:T(8,128)(2,1)S(1)} %get-tuple-element.41), channel_id=1, source_target_pairs={{0,12},{4,8},{8,4},{12,0},{1,13},{5,9},{9,5},{13,1},{2,14},{6,10},... | collective-permute-start | bytes 786440 | tf_op jit(solution)/shard_map/ppermute | solution.py:214
  10.6 16.3 %copy-start.12 = (bf16[4,256,4]{1,2,0:T(4,128)(2,1)S(1)}, bf16[4,256,4]{1,2,0:T(4,128)(2,1)}, u32[]{:S(2)}) copy-start(bf16[4,256,4]{1,2,0:T(4,128)(2,1)} %param.10) | copy-start | bytes 24580
  17.5 16.4 %copy-start.3 = (bf16[256,512]{1,0:T(8,128)(2,1)}, bf16[256,512]{1,0:T(8,128)(2,1)S(1)}, u32[]{:S(2)}) copy-start(bf16[256,512]{1,0:T(8,128)(2,1)S(1)} %collective-permute-done.1.refs_1_) | copy-start | bytes 786436
  17.5 9.2 %collective-permute-start.3 = (bf16[256,512]{1,0:T(8,128)(2,1)S(1)}, bf16[256,512]{1,0:T(8,128)(2,1)S(1)}, u32[]{:S(2)}, u32[]{:S(2)}) collective-permute-start(bf16[256,512]{1,0:T(8,128)(2,1)S(1)} %collective-permute-done.1.refs_1_), channel_id=1, source_target_pairs={{0,2},{1,3},{2,0},{3,1},{4,6},{5,7},{6,4},{7,5},{8,10},{9,11},{10,... | collective-permute-start | bytes 786440 | tf_op jit(solution)/shard_map/ppermute | solution.py:214
  19.2 22.2 %copy-start.1 = (bf16[256,512]{1,0:T(8,128)(2,1)}, bf16[256,512]{1,0:T(8,128)(2,1)S(1)}, u32[]{:S(2)}) copy-start(bf16[256,512]{1,0:T(8,128)(2,1)S(1)} %collective-permute-done.8.refs_1_) | copy-start | bytes 786436
  19.2 14.2 %collective-permute-start.10 = (bf16[256,512]{1,0:T(8,128)(2,1)S(1)}, bf16[256,512]{1,0:T(8,128)(2,1)S(1)}, u32[]{:S(2)}, u32[]{:S(2)}) collective-permute-start(bf16[256,512]{1,0:T(8,128)(2,1)S(1)} %collective-permute-done.8.refs_1_), channel_id=1, source_target_pairs={{0,2},{1,3},{2,0},{3,1},{4,6},{5,7},{6,4},{7,5},{8,10},{9,11},{10,... | collective-permute-start | bytes 786440 | tf_op jit(solution)/shard_map/ppermute | solution.py:214
  20.7 13.2 %collective-permute-start.2 = (bf16[256,512]{1,0:T(8,128)(2,1)S(1)}, bf16[256,512]{1,0:T(8,128)(2,1)S(1)}, u32[]{:S(2)}, u32[]{:S(2)}) collective-permute-start(bf16[256,512]{1,0:T(8,128)(2,1)S(1)} %collective-permute-done.1.refs_1_), channel_id=1, source_target_pairs={{0,1},{1,0},{2,3},{3,2},{4,5},{5,4},{6,7},{7,6},{8,9},{9,8},{10,11... | collective-permute-start | bytes 786440 | tf_op jit(solution)/shard_map/ppermute | solution.py:214
  26.7 7.2 %copy-start.6 = (bf16[256,512]{1,0:T(8,128)(2,1)}, bf16[256,512]{1,0:T(8,128)(2,1)S(1)}, u32[]{:S(2)}) copy-start(bf16[256,512]{1,0:T(8,128)(2,1)S(1)} %collective-permute-done.3.refs_3_) | copy-start | bytes 786436
  26.7 7.1 %collective-permute-start.4 = (bf16[256,512]{1,0:T(8,128)(2,1)S(1)}, bf16[256,512]{1,0:T(8,128)(2,1)S(1)}, u32[]{:S(2)}, u32[]{:S(2)}) collective-permute-start(bf16[256,512]{1,0:T(8,128)(2,1)S(1)} %collective-permute-done.3.refs_3_), channel_id=1, source_target_pairs={{0,1},{1,0},{2,3},{3,2},{4,5},{5,4},{6,7},{7,6},{8,9},{9,8},{10,11... | collective-permute-start | bytes 786440 | tf_op jit(solution)/shard_map/ppermute | solution.py:214
  26.7 15.2 %collective-permute-start = (bf16[256,512]{1,0:T(8,128)(2,1)S(1)}, bf16[256,512]{1,0:T(8,128)(2,1)S(1)}, u32[]{:S(2)}, u32[]{:S(2)}) collective-permute-start(bf16[256,512]{1,0:T(8,128)(2,1)S(1)} %get-tuple-element.43), channel_id=1, source_target_pairs={{0,8},{4,12},{8,0},{12,4},{1,9},{5,13},{9,1},{13,5},{2,10},{6,14},... | collective-permute-start | bytes 786440 | tf_op jit(solution)/shard_map/ppermute | solution.py:214
  26.8 6.5 %collective-permute-start.5 = (bf16[4,256]{1,0:T(4,128)(2,1)S(1)}, bf16[4,256]{1,0:T(4,128)(2,1)S(1)}, u32[]{:S(2)}, u32[]{:S(2)}) collective-permute-start(bf16[4,256]{1,0:T(4,128)(2,1)S(1)} %get-tuple-element.45), channel_id=1, source_target_pairs={{0,4},{4,0},{8,12},{12,8},{1,5},{5,1},{9,13},{13,9},{2,6},{6,2},{1... | collective-permute-start | bytes 6152 | tf_op jit(solution)/shard_map/ppermute | solution.py:214
  33.3 0.6 copy-start.14
  33.3 15.5 %collective-permute-start.9 = (bf16[256,512]{1,0:T(8,128)(2,1)S(1)}, bf16[256,512]{1,0:T(8,128)(2,1)S(1)}, u32[]{:S(2)}, u32[]{:S(2)}) collective-permute-start(bf16[256,512]{1,0:T(8,128)(2,1)S(1)} %collective-permute-done.8.refs_1_), channel_id=1, source_target_pairs={{0,1},{1,0},{2,3},{3,2},{4,5},{5,4},{6,7},{7,6},{8,9},{9,8},{10,11... | collective-permute-start | bytes 786440 | tf_op jit(solution)/shard_map/ppermute | solution.py:214
  33.3 8.0 %copy-start.2 = (bf16[256,512]{1,0:T(8,128)(2,1)}, bf16[256,512]{1,0:T(8,128)(2,1)S(1)}, u32[]{:S(2)}) copy-start(bf16[256,512]{1,0:T(8,128)(2,1)S(1)} %collective-permute-done.10.refs_3_) | copy-start | bytes 786436
  33.3 15.5 %collective-permute-start.11 = (bf16[256,512]{1,0:T(8,128)(2,1)S(1)}, bf16[256,512]{1,0:T(8,128)(2,1)S(1)}, u32[]{:S(2)}, u32[]{:S(2)}) collective-permute-start(bf16[256,512]{1,0:T(8,128)(2,1)S(1)} %collective-permute-done.10.refs_3_), channel_id=1, source_target_pairs={{0,1},{1,0},{2,3},{3,2},{4,5},{5,4},{6,7},{7,6},{8,9},{9,8},{10,11... | collective-permute-start | bytes 786440 | tf_op jit(solution)/shard_map/ppermute | solution.py:214
  33.9 0.7 copy-start.8
  33.9 0.8 %copy-start.10 = (bf16[256,512]{1,0:T(8,128)(2,1)}, bf16[256,512]{1,0:T(8,128)(2,1)S(1)}, u32[]{:S(2)}) copy-start(bf16[256,512]{1,0:T(8,128)(2,1)S(1)} %collective-permute-done.4.refs_4_) | copy-start | bytes 786436
  42.0 14.4 %copy-start = (bf16[256,512]{1,0:T(8,128)(2,1)}, bf16[256,512]{1,0:T(8,128)(2,1)S(1)}, u32[]{:S(2)}) copy-start(bf16[256,512]{1,0:T(8,128)(2,1)S(1)} %collective-permute-done.refs_1_) | copy-start | bytes 786436
  42.0 14.4 %collective-permute-start.7 = (bf16[256,512]{1,0:T(8,128)(2,1)S(1)}, bf16[256,512]{1,0:T(8,128)(2,1)S(1)}, u32[]{:S(2)}, u32[]{:S(2)}) collective-permute-start(bf16[256,512]{1,0:T(8,128)(2,1)S(1)} %collective-permute-done.refs_1_), channel_id=1, source_target_pairs={{0,2},{1,3},{2,0},{3,1},{4,6},{5,7},{6,4},{7,5},{8,10},{9,11},{10,... | collective-permute-start | bytes 786440 | tf_op jit(solution)/shard_map/ppermute | solution.py:214
  43.4 5.4 %collective-permute-start.12 = (bf16[4,256]{1,0:T(4,128)(2,1)S(1)}, bf16[4,256]{1,0:T(4,128)(2,1)S(1)}, u32[]{:S(2)}, u32[]{:S(2)}) collective-permute-start(bf16[4,256]{1,0:T(4,128)(2,1)S(1)} %get-tuple-element.46), channel_id=1, source_target_pairs={{0,12},{4,8},{8,4},{12,0},{1,13},{5,9},{9,5},{13,1},{2,14},{6,10},... | collective-permute-start | bytes 6152 | tf_op jit(solution)/shard_map/ppermute | solution.py:214
  46.3 14.7 %collective-permute-start.6 = (bf16[256,512]{1,0:T(8,128)(2,1)S(1)}, bf16[256,512]{1,0:T(8,128)(2,1)S(1)}, u32[]{:S(2)}, u32[]{:S(2)}) collective-permute-start(bf16[256,512]{1,0:T(8,128)(2,1)S(1)} %collective-permute-done.refs_1_), channel_id=1, source_target_pairs={{0,1},{1,0},{2,3},{3,2},{4,5},{5,4},{6,7},{7,6},{8,9},{9,8},{10,11... | collective-permute-start | bytes 786440 | tf_op jit(solution)/shard_map/ppermute | solution.py:214
  48.8 0.6 copy-start.15
  48.8 0.7 copy-start.7
  48.8 0.8 %copy-start.9 = (bf16[256,512]{1,0:T(8,128)(2,1)}, bf16[256,512]{1,0:T(8,128)(2,1)S(1)}, u32[]{:S(2)}) copy-start(bf16[256,512]{1,0:T(8,128)(2,1)S(1)} %collective-permute-done.11.refs_4_) | copy-start | bytes 786436
  56.4 4.7 %copy-start.4 = (bf16[256,512]{1,0:T(8,128)(2,1)}, bf16[256,512]{1,0:T(8,128)(2,1)S(1)}, u32[]{:S(2)}) copy-start(bf16[256,512]{1,0:T(8,128)(2,1)S(1)} %collective-permute-done.7.refs_3_) | copy-start | bytes 786436
  56.4 4.6 %collective-permute-start.13 = (bf16[256,512]{1,0:T(8,128)(2,1)S(1)}, bf16[256,512]{1,0:T(8,128)(2,1)S(1)}, u32[]{:S(2)}, u32[]{:S(2)}) collective-permute-start(bf16[256,512]{1,0:T(8,128)(2,1)S(1)} %collective-permute-done.7.refs_3_), channel_id=1, source_target_pairs={{0,1},{1,0},{2,3},{3,2},{4,5},{5,4},{6,7},{7,6},{8,9},{9,8},{10,11... | collective-permute-start | bytes 786440 | tf_op jit(solution)/shard_map/ppermute | solution.py:214
  56.4 4.5 %collective-permute-start.14 = (bf16[4,256]{1,0:T(4,128)(2,1)S(1)}, bf16[4,256]{1,0:T(4,128)(2,1)S(1)}, u32[]{:S(2)}, u32[]{:S(2)}) collective-permute-start(bf16[4,256]{1,0:T(4,128)(2,1)S(1)} %get-tuple-element.44), channel_id=1, source_target_pairs={{0,8},{4,12},{8,0},{12,4},{1,9},{5,13},{9,1},{13,5},{2,10},{6,14},... | collective-permute-start | bytes 6152 | tf_op jit(solution)/shard_map/ppermute | solution.py:214
  61.0 0.6 copy-start.13
  61.0 0.7 copy-start.5
  61.0 0.8 %copy-start.11 = (bf16[256,512]{1,0:T(8,128)(2,1)}, bf16[256,512]{1,0:T(8,128)(2,1)S(1)}, u32[]{:S(2)}) copy-start(bf16[256,512]{1,0:T(8,128)(2,1)S(1)} %collective-permute-done.13.refs_4_) | copy-start | bytes 786436
  61.8 6.7 %copy-start.16 = (f32[1,512]{1,0:T(1,128)S(1)}, f32[1,512]{1,0:T(1,128)}, u32[]{:S(2)}) copy-start(f32[1,512]{1,0:T(1,128)} %get-tuple-element.36) | copy-start | bytes 6148
  61.8 6.7 %copy-start.17 = (f32[1,512]{1,0:T(1,128)S(1)}, f32[1,512]{1,0:T(1,128)}, u32[]{:S(2)}) copy-start(f32[1,512]{1,0:T(1,128)} %get-tuple-element.22) | copy-start | bytes 6148
  61.8 6.7 %copy-start.18 = (f32[1,512]{1,0:T(1,128)S(1)}, f32[1,512]{1,0:T(1,128)}, u32[]{:S(2)}) copy-start(f32[1,512]{1,0:T(1,128)} %get-tuple-element.38) | copy-start | bytes 6148
  61.8 6.7 %copy-start.19 = (f32[1,512]{1,0:T(1,128)S(1)}, f32[1,512]{1,0:T(1,128)}, u32[]{:S(2)}) copy-start(f32[1,512]{1,0:T(1,128)} %get-tuple-element.26) | copy-start | bytes 6148
  61.8 6.8 %copy-start.20 = (f32[1,512]{1,0:T(1,128)S(1)}, f32[1,512]{1,0:T(1,128)}, u32[]{:S(2)}) copy-start(f32[1,512]{1,0:T(1,128)} %get-tuple-element.39) | copy-start | bytes 6148
  61.9 6.8 %copy-start.21 = (f32[1,512]{1,0:T(1,128)S(1)}, f32[1,512]{1,0:T(1,128)}, u32[]{:S(2)}) copy-start(f32[1,512]{1,0:T(1,128)} %get-tuple-element.30) | copy-start | bytes 6148
  69.3 4.5 %collective-permute-start.15 = (f32[1,512]{1,0:T(1,128)S(1)}, f32[1,512]{1,0:T(1,128)S(1)}, u32[]{:S(2)}, u32[]{:S(2)}) collective-permute-start(f32[1,512]{1,0:T(1,128)S(1)} %multiply_add_fusion), channel_id=1, source_target_pairs={{0,8},{4,12},{8,0},{12,4},{1,9},{5,13},{9,1},{13,5},{2,10},{6,14},... | collective-permute-start | bytes 6152 | tf_op jit(solution)/shard_map/ppermute | solution.py:214
  70.9 5.4 %collective-permute-start.16 = (f32[1,512]{1,0:T(1,128)S(1)}, f32[1,512]{1,0:T(1,128)S(1)}, u32[]{:S(2)}, u32[]{:S(2)}) collective-permute-start(f32[1,512]{1,0:T(1,128)S(1)} %multiply_add_fusion), channel_id=1, source_target_pairs={{0,12},{4,8},{8,4},{12,0},{1,13},{5,9},{9,5},{13,1},{2,14},{6,10},... | collective-permute-start | bytes 6152 | tf_op jit(solution)/shard_map/ppermute | solution.py:214
  71.9 4.3 %collective-permute-start.17 = (f32[1,512]{1,0:T(1,128)S(1)}, f32[1,512]{1,0:T(1,128)S(1)}, u32[]{:S(2)}, u32[]{:S(2)}) collective-permute-start(f32[1,512]{1,0:T(1,128)S(1)} %multiply_add_fusion), channel_id=1, source_target_pairs={{0,4},{4,0},{8,12},{12,8},{1,5},{5,1},{9,13},{13,9},{2,6},{6,2},{1... | collective-permute-start | bytes 6152 | tf_op jit(solution)/shard_map/ppermute | solution.py:214

commit v3 on v2

--- a/solution.py
+++ b/solution.py
@@ -82,8 +82,10 @@
 def block_kernel(part_count, whole_rows, carried, *refs):
     index_ref = refs[0]
     parts = refs[1 : 1 + part_count]
-    gain_ref, key_ref, value_ref, bias_ref, query_ref = refs[1 + part_count : 6 + part_count]
-    rest = refs[6 + part_count + (2 if carried else 0) :]
+    gain_ref, key_ref, value_ref, query_ref = refs[1 + part_count : 5 + part_count]
+    after_query = 5 + part_count
+    bias_ref = None if carried else refs[after_query]
+    rest = refs[after_query + (2 if carried else 1) :]
     cache_ref, bias_out_ref, partial_ref, total_ref = rest[:4]
     normed_ref, key_local, value_local, weight_sems = rest[4:]
     key_copy = pltpu.make_async_copy(key_ref, key_local, weight_sems.at[0])
@@ -91,7 +93,7 @@
     key_copy.start()
     value_copy.start()
     piece, width = normed_ref.shape
-    heads_here = bias_ref.shape[-2]
+    heads_here = bias_out_ref.shape[-2]
     columns = key_ref.shape[1]
     head_size = columns // heads_here
     gain = gain_ref[...].astype(jnp.float32)
@@ -104,13 +106,13 @@
         share = width // part_count
         square_sum = jnp.zeros((piece, 1), jnp.float32)
         for part in parts:
-            widened = part[...].astype(jnp.float32)
+            widened = part[:piece].astype(jnp.float32)
             square_sum = square_sum + jnp.sum(widened * widened, axis=-1, keepdims=True)
         inverse = lax.rsqrt(square_sum * (1.0 / width) + norm_eps)
         for offset, part in enumerate(parts):
             start = pl.multiple_of((index_ref[1] ^ offset) * share, share)
             own_gain = gain_ref[:, pl.ds(start, share)].astype(jnp.float32)
-            scaled = part[...].astype(jnp.float32) * inverse * own_gain
+            scaled = part[:piece].astype(jnp.float32) * inverse * own_gain
             normed_ref[:, pl.ds(start, share)] = scaled.astype(jnp.bfloat16)
     normed = normed_ref[...]
     key_copy.wait()
@@ -122,8 +124,11 @@
         jnp.bfloat16
     )
     cache_ref[0, 0] = jnp.stack((key_rows, value_rows), axis=1)
-    bias = bias_ref[...].reshape(heads_here, piece)
-    bias_out_ref[0] = bias
+    if carried:
+        bias = parts[0][piece:, :piece].astype(jnp.float32)[:heads_here]
+    else:
+        bias = bias_ref[0].astype(jnp.float32)
+    bias_out_ref[0] = bias.astype(jnp.bfloat16)
     head_of_row = lax.broadcasted_iota(jnp.int32, (heads_here, columns), 0)
     head_of_column = lax.broadcasted_iota(jnp.int32, (heads_here, columns), 1) // head_size
     own_head = head_of_row == head_of_column
@@ -131,7 +136,7 @@
     logits = lax.dot_general(
         query, key_rows, (((1,), (1,)), ((), ())), preferred_element_type=jnp.float32
     )
-    logits = logits * head_size ** (-0.5) + bias.astype(jnp.float32)
+    logits = logits * head_size ** (-0.5) + bias
     soft = jnp.log1p(jnp.exp(-jnp.abs(logits)))
     keep_log = jnp.minimum(-logits, 0.0) - soft
     break_log = jnp.minimum(logits, 0.0) - soft
@@ -150,11 +155,10 @@
     total_ref[...] = jnp.sum(jnp.where(own_head, totals, 0.0), axis=0, keepdims=True)
 
 
-def build_block(index, parts, gain, key_weight, value_weight, bias, query, carried, block_count):
+def build_block(index, parts, gain, key_weight, value_weight, bias, query, carried):
     whole_rows = parts[0].ndim == 3
     width, columns = key_weight.shape
-    piece = parts[0].shape[-2]
-    heads_here = bias.shape[-2]
+    block_count, heads_here, piece = bias.shape
     part_count = len(parts)
 
     def full(array):
@@ -162,15 +166,16 @@
 
     if whole_rows:
         part_specs = [pl.BlockSpec((1, piece, width), lambda g, s: (s[0], 0, 0))]
-        bias_spec = pl.BlockSpec((1, heads_here, piece), lambda g, s: (s[0], 0, 0))
     else:
         part_specs = [full(part) for part in parts]
-        bias_spec = full(bias)
-    operands = [index, *parts, gain, key_weight, value_weight, bias, query]
+    operands = [index, *parts, gain, key_weight, value_weight, query]
     in_place = pl.BlockSpec(memory_space=pl.ANY)
-    specs = part_specs + [full(gain), in_place, in_place, bias_spec, full(query)]
+    specs = part_specs + [full(gain), in_place, in_place, full(query)]
     aliases = {}
-    if carried is not None:
+    if carried is None:
+        operands.append(bias)
+        specs.append(pl.BlockSpec((1, heads_here, piece), lambda g, s: (s[0], 0, 0)))
+    else:
         aliases = {len(operands): 0, len(operands) + 1: 1}
         operands += list(carried)
         specs += [in_place] * 2
@@ -201,12 +206,16 @@
             row,
         ],
         input_output_aliases=aliases,
+        compiler_params=pltpu.CompilerParams(vmem_limit_bytes=24 * 1024 * 1024),
         cost_estimate=pl.CostEstimate(
             flops=4 * piece * width * columns,
             transcendentals=3 * heads_here * piece,
             bytes_accessed=4 * width * columns + 2 * piece * (width + 2 * columns),
         ),
     )(*operands)
+
+
+bias_tile = 16
 
 
 def swap(array, axis, offset):
@@ -230,6 +239,7 @@
     own = lax.axis_index("sp")
     own_share = lax.axis_index("tp")
     bias_rows = jnp.transpose(break_bias, (0, 2, 1))
+    heads_here = bias_rows.shape[1]
     columns = key_weight.shape[1]
     gain = norm_gain.reshape(1, width)
     query = lax.dynamic_slice_in_dim(new_query, own, 1, 0).astype(jnp.float32)
@@ -239,15 +249,14 @@
 
     order = exchange_order(block_count)
     arrived = {}
-    bias_arrived = {}
     for offset in order:
         sent = lax.dynamic_slice(
             tokens, (own ^ offset, 0, own_share * share), (1, piece, share)
         ).reshape(piece, share)
+        bias_sent = lax.dynamic_index_in_dim(bias_rows, own ^ offset, 0, False)
+        bias_sent = jnp.pad(bias_sent, ((0, bias_tile - heads_here), (0, share - piece)))
+        sent = jnp.concatenate((sent, bias_sent), axis=0)
         arrived[offset] = swap(sent, "sp", offset)
-    for offset in order:
-        bias_sent = lax.dynamic_index_in_dim(bias_rows, own ^ offset, 0, False)
-        bias_arrived[offset] = swap(bias_sent, "sp", offset)
     built = {}
     built[0] = build_block(
         index_of(0),
@@ -258,13 +267,12 @@
         bias_rows,
         query,
         None,
-        block_count,
     )
     latest = built[0]
     for place, offset in enumerate(order):
         shares = {0: arrived[offset]}
-        if place != 1:
-            shares[0] = after(shares[0], built[order[place - 2] if place else 0])
+        if place > 1:
+            shares[0] = after(shares[0], built[order[place - 2]])
         bit = share_count // 2
         while bit:
             for known in list(shares):
@@ -280,10 +288,9 @@
             gain,
             key_weight,
             value_weight,
-            bias_arrived[offset],
+            bias_rows,
             query,
             latest[:2],
-            block_count,
         )
         built[offset] = latest
     cache_pair, cache_bias = latest[:2]
@@ -308,6 +315,8 @@
     paired = block_count & (block_count - 1) == 0 and share_count & (share_count - 1) == 0
     aligned = width % (128 * share_count) == 0
     whole_prompt = seq_count == block_count and block_count > 1
+    whole_prompt = whole_prompt and tokens.shape[1] <= width // share_count
+    whole_prompt = whole_prompt and break_bias.shape[2] <= bias_tile
     body = exchange_tokens if paired and aligned and whole_prompt else exchange_rows
     return body(tokens, norm_gain, key_weight, value_weight, break_bias, new_query)
 

time: 77.3 us -> 68.9 us (0.89)
  Pallas kernels: 26.9 us -> 17.8 us
  other arithmetic: 5.02 us -> 1.8 us
  local copies, waits for them, and re-layouts: 4.9 us -> 7.43 us
  starting transfers between devices: 21.1 us -> 23.5 us
  waiting for transfers between devices: 18.1 us -> 17.3 us
    pallas_call x4, Pallas kernels: 26.9 us -> 17.8 us  [build_block(): pl.pallas_call(functools.partial(block_kernel, part_count, whole_rows, ca...]
    unnamed x44 -> x16, local copies, waits for them, and re-layouts: 2.43 us -> 5.39 us
    ppermute x18 -> x15, starting transfers between devices: 21.1 us -> 23.5 us  [swap(): return lax.ppermute(array, axis, [(k, k ^ offset) for k in range(size)])]
    another operation x4, other arithmetic: 2.33 us -> 0.3 us  [index_of(): return jnp.stack((own ^ offset, own_share)).astype(jnp.int32)]
    reshape x1, local copies, waits for them, and re-layouts: 1.29 us -> 0.01 us  [exchange_tokens(): gain = norm_gain.reshape(1, width)]
    convert_element_type x1, other arithmetic: 1.28 us -> 0.01 us  [exchange_tokens(): query = lax.dynamic_slice_in_dim(new_query, own, 1, 0).astype(jnp.float32)]
    squeeze x1, local copies, waits for them, and re-layouts: 0.01 us -> 0.87 us  [exchange_tokens(): bias_sent = lax.dynamic_index_in_dim(bias_rows, own ^ offset, 0, False)]
    ppermute x18 -> x15, waiting for transfers between devices: 18.1 us -> 17.3 us  [swap(): return lax.ppermute(array, axis, [(k, k ^ offset) for k in range(size)])]
  transfers between devices with their start and end apart: 18 -> 15, of which waited for: 8 -> 6; matrix products, arithmetic and copies ran while one was open for 6% -> 2% of each run, Pallas kernels for 26% -> 19%
where the time goes in v3:
time: 68.9 us; the launch traced here: 68.6 us
  starting transfers between devices  23.5 us (34%)
  Pallas kernels  17.8 us (26%)
  waiting for transfers between devices  17.3 us (25%)
  local copies, waits for them, and re-layouts  7.43 us (11%)
  other arithmetic  1.8 us (3%)
  between operations  0.8 us (1%)
    ppermute x15, starting transfers between devices, swap(): return lax.ppermute(array, axis, [(k, k ^ offset) for k in range(size)])  23.5 us
    pallas_call x4, Pallas kernels, build_block(): pl.pallas_call(functools.partial(block_kernel, part_count, whole_rows, ca...  17.8 us
    ppermute x15, waiting for transfers between devices, swap(): return lax.ppermute(array, axis, [(k, k ^ offset) for k in range(size)])  17.3 us
    unnamed x16, local copies, waits for them, and re-layouts  5.39 us
  transfers between devices with their start and end apart: 15, of which 6 were waited for; matrix products, arithmetic and copies ran while one was open for 2% of the time, Pallas kernels for 19%

profile of v3, /device:TPU:0, one launch (start us, length us, event | category | flops | bytes accessed | tf_op | source)
XLA Modules:
  0.0 68.6 jit_solution(4396707466363712468)
XLA Ops:
  0.6 0.0 copy-start.5
  0.7 0.9 %dynamic-slice_bitcast_fusion.3 = (bf16[4,256]{1,0:T(4,128)(2,1)S(1)}, bf16[4,256]{1,0:T(4,128)(2,1)S(1)}, bf16[4,256]{1,0:T(4,128)(2,1)S(1)}) fusion(bf16[4,256,4]{1,2,0:T(4,128)(2,1)} %param.10, s32[]{:T(128)S(6)} %select_n.113, s32[]{:T(128)S(6)} %select_n.111, s32[]{:T(128)S(6)} %select_n.109), kind=kLoop, calls=%fused_computation.32 | loop fusion | bytes 12300 | tf_op jit(solution)/shard_map/jit(dynamic_index_in_dim)/squeeze | solution.py:256
  1.6 1.2 %dynamic-slice_bitcast_fusion = (bf16[256,512]{1,0:T(8,128)(2,1)S(1)}, bf16[256,512]{1,0:T(8,128)(2,1)S(1)}, bf16[256,512]{1,0:T(8,128)(2,1)S(1)}) fusion(bf16[4,256,2048]{2,1,0:T(8,128)(2,1)} %refs_1_.1, s32[]{:T(128)S(6)} %select_n.113, s32[]{:T(128)S(6)} %select_n.110, s32[]{:T(128)S(6)} %select_n.111, s32[]{:T(128)S(6)} %select_n.109), kind=kLoop, calls=%fused_computation.7 | loop fusion | bytes 1572880 | tf_op jit(solution)/shard_map/reshape | solution.py:255
  2.8 3.1 %collective-permute-start.1 = (bf16[272,512]{1,0:T(8,128)(2,1)S(1)}, bf16[272,512]{1,0:T(8,128)(2,1)S(1)}, u32[]{:S(2)}, u32[]{:S(2)}) collective-permute-start(bf16[272,512]{1,0:T(8,128)(2,1)S(1)} %fusion.4), channel_id=1, source_target_pairs={{0,4},{4,0},{8,12},{12,8},{1,5},{5,1},{9,13},{13,9},{2,6},{6,2},{1... | collective-permute-start | bytes 835592 | tf_op jit(solution)/shard_map/ppermute | solution.py:223
  5.9 0.7 %fusion.5 = bf16[272,512]{1,0:T(8,128)(2,1)} fusion(bf16[4,256]{1,0:T(4,128)(2,1)S(1)} %get-tuple-element.42, bf16[256,512]{1,0:T(8,128)(2,1)S(1)} %get-tuple-element.39), kind=kLoop, calls=%fused_computation.6 | loop fusion | flops 835584 | bytes 542720 | tf_op jit(solution)/shard_map/concatenate | solution.py:258
  6.6 2.5 %collective-permute-start.7 = (bf16[272,512]{1,0:T(8,128)(2,1)}, bf16[272,512]{1,0:T(8,128)(2,1)S(1)}, u32[]{:S(2)}, u32[]{:S(2)}) collective-permute-start(bf16[272,512]{1,0:T(8,128)(2,1)} %fusion.5), channel_id=1, source_target_pairs={{0,12},{4,8},{8,4},{12,0},{1,13},{5,9},{9,5},{13,1},{2,14},{6,10},... | collective-permute-start | bytes 835592 | tf_op jit(solution)/shard_map/ppermute | solution.py:223
  9.1 3.8 %collective-permute-done.1.refs_1_ = bf16[272,512]{1,0:T(8,128)(2,1)S(1)} collective-permute-done((bf16[272,512]{1,0:T(8,128)(2,1)S(1)}, bf16[272,512]{1,0:T(8,128)(2,1)S(1)}, u32[]{:S(2)}, u32[]{:S(2)}) %collective-permute-start.1) | collective-permute-done | bytes 278560 | tf_op jit(solution)/shard_map/ppermute | solution.py:223
  12.9 1.5 %collective-permute-start.3 = (bf16[272,512]{1,0:T(8,128)(2,1)S(1)}, bf16[272,512]{1,0:T(8,128)(2,1)S(1)}, u32[]{:S(2)}, u32[]{:S(2)}) collective-permute-start(bf16[272,512]{1,0:T(8,128)(2,1)S(1)} %collective-permute-done.1.refs_1_), channel_id=1, source_target_pairs={{0,2},{1,3},{2,0},{3,1},{4,6},{5,7},{6,4},{7,5},{8,10},{9,11},{10,... | collective-permute-start | bytes 835592 | tf_op jit(solution)/shard_map/ppermute | solution.py:223
  14.4 3.6 %collective-permute-start = (bf16[272,512]{1,0:T(8,128)(2,1)S(1)}, bf16[272,512]{1,0:T(8,128)(2,1)S(1)}, u32[]{:S(2)}, u32[]{:S(2)}) collective-permute-start(bf16[272,512]{1,0:T(8,128)(2,1)S(1)} %fusion.3), channel_id=1, source_target_pairs={{0,8},{4,12},{8,0},{12,4},{1,9},{5,13},{9,1},{13,5},{2,10},{6,14},... | collective-permute-start | bytes 835592 | tf_op jit(solution)/shard_map/ppermute | solution.py:223
  18.0 0.0 copy-done.6
  18.0 0.1 collective-permute-start.2
  18.1 3.8 %collective-permute-done.7.refs_1_ = bf16[272,512]{1,0:T(8,128)(2,1)S(1)} collective-permute-done((bf16[272,512]{1,0:T(8,128)(2,1)}, bf16[272,512]{1,0:T(8,128)(2,1)S(1)}, u32[]{:S(2)}, u32[]{:S(2)}) %collective-permute-start.7) | collective-permute-done | bytes 278560 | tf_op jit(solution)/shard_map/ppermute | solution.py:223
  21.9 1.5 %collective-permute-start.9 = (bf16[272,512]{1,0:T(8,128)(2,1)S(1)}, bf16[272,512]{1,0:T(8,128)(2,1)S(1)}, u32[]{:S(2)}, u32[]{:S(2)}) collective-permute-start(bf16[272,512]{1,0:T(8,128)(2,1)S(1)} %collective-permute-done.7.refs_1_), channel_id=1, source_target_pairs={{0,2},{1,3},{2,0},{3,1},{4,6},{5,7},{6,4},{7,5},{8,10},{9,11},{10,... | collective-permute-start | bytes 835592 | tf_op jit(solution)/shard_map/ppermute | solution.py:223
  23.4 0.0 collective-permute-done.3.refs_3_
  23.4 0.0 collective-permute-start.4
  23.4 0.1 pad_add_fusion.2.refs_0_
  23.5 0.0 copy-done.5
  23.5 1.6 %copy-done.1 = bf16[2048,512]{1,0:T(8,128)(2,1)S(1)} copy-done((bf16[2048,512]{1,0:T(8,128)(2,1)S(1)}, bf16[2048,512]{1,0:T(8,128)(2,1)}, u32[]{:S(2)}) %copy-start.1) | copy-done | bytes 2097176
  25.1 2.2 %copy-done.4 = bf16[4,256,2048]{2,1,0:T(8,128)(2,1)S(1)} copy-done((bf16[4,256,2048]{2,1,0:T(8,128)(2,1)S(1)}, bf16[4,256,2048]{2,1,0:T(8,128)(2,1)}, u32[]{:S(2)}) %copy-start.4) | copy-done | bytes 4194328
  27.3 4.3 %shard_map.85 = (bf16[1,4,256,2,512]{4,3,2,1,0:T(2,128)(2,1)}, bf16[4,4,256]{2,1,0:T(4,128)(2,1)}, f32[1,512]{1,0:T(1,128)S(1)}, f32[1,512]{1,0:T(1,128)S(1)}) custom-call(s32[2]{0:T(128)S(1)} %pad_add_fusion.2.refs_0_, bf16[4,256,2048]{2,1,0:T(8,128)(2,1)S(1)} %copy-done.4, bf16[1,2048]{1,0:T(2,128)(2,1)S(1)} %reshape.40.refs_2_.refs_5_, ...), custom_call_target="tpu_custom_call" | custom-call | flops 1073741824 | bytes 5767168 | tf_op jit(solution)/shard_map/pallas_call | solution.py:183
  31.6 0.1 pad_add_fusion.1.refs_0_
  31.7 0.5 collective-permute-start.8
  32.2 0.0 collective-permute-done.9.refs_3_
  32.2 0.1 collective-permute-start.10
  32.3 0.0 collective-permute-done.2.refs_2_
  32.3 0.0 collective-permute-done.4.refs_4_
  32.3 4.5 %shard_map.86 = (bf16[1,4,256,2,512]{4,3,2,1,0:T(2,128)(2,1)}, bf16[4,4,256]{2,1,0:T(4,128)(2,1)}, f32[1,512]{1,0:T(1,128)S(1)}, f32[1,512]{1,0:T(1,128)S(1)}) custom-call(s32[2]{0:T(128)S(1)} %pad_add_fusion.1.refs_0_, bf16[272,512]{1,0:T(8,128)(2,1)S(1)} %collective-permute-done.1.refs_1_, ...), custom_call_target="tpu_custom_call", output_to_operand_aliasing={{0}: (9, {}), {1}: (10, {})} | custom-call | flops 1073741824 | bytes 5767168 | tf_op jit(solution)/shard_map/pallas_call | solution.py:183
  36.8 0.0 collective-permute-done.refs_1_
  36.8 0.6 collective-permute-start.6
  37.4 0.1 pad_add_fusion.3.refs_0_
  37.5 0.1 collective-permute-start.5
  37.6 0.0 collective-permute-done.8.refs_2_
  37.6 0.0 collective-permute-done.10.refs_4_
  37.7 4.5 %shard_map.87 = (bf16[1,4,256,2,512]{4,3,2,1,0:T(2,128)(2,1)}, bf16[4,4,256]{2,1,0:T(4,128)(2,1)}, f32[1,512]{1,0:T(1,128)S(1)}, f32[1,512]{1,0:T(1,128)S(1)}) custom-call(s32[2]{0:T(128)S(1)} %pad_add_fusion.3.refs_0_, bf16[272,512]{1,0:T(8,128)(2,1)S(1)} %collective-permute-done.7.refs_1_, ...), custom_call_target="tpu_custom_call", output_to_operand_aliasing={{0}: (9, {}), {1}: (10, {})} | custom-call | flops 1073741824 | bytes 5767168 | tf_op jit(solution)/shard_map/pallas_call | solution.py:183
  42.1 3.7 %collective-permute-done.6.refs_3_ = bf16[272,512]{1,0:T(8,128)(2,1)S(1)} collective-permute-done((bf16[272,512]{1,0:T(8,128)(2,1)S(1)}, bf16[272,512]{1,0:T(8,128)(2,1)S(1)}, u32[]{:S(2)}, u32[]{:S(2)}) %collective-permute-start.6) | collective-permute-done | bytes 278560 | tf_op jit(solution)/shard_map/ppermute | solution.py:223
  45.9 0.0 collective-permute-start.11
  45.9 0.1 pad_add_fusion.refs_0_
  46.0 0.0 collective-permute-done.5.refs_2_
  46.0 1.5 %collective-permute-done.11.refs_4_ = bf16[272,512]{1,0:T(8,128)(2,1)S(1)} collective-permute-done((bf16[272,512]{1,0:T(8,128)(2,1)S(1)}, bf16[272,512]{1,0:T(8,128)(2,1)S(1)}, u32[]{:S(2)}, u32[]{:S(2)}) %collective-permute-start.11) | collective-permute-done | bytes 278560 | tf_op jit(solution)/shard_map/ppermute | solution.py:223
  47.4 1.6 %copy-done.3 = bf16[2048,512]{1,0:T(8,128)(2,1)S(1)} copy-done((bf16[2048,512]{1,0:T(8,128)(2,1)S(1)}, bf16[2048,512]{1,0:T(8,128)(2,1)}, u32[]{:S(2)}) %copy-start.3) | copy-done | bytes 2097176
  49.0 4.5 %shard_map.88 = (bf16[1,4,256,2,512]{4,3,2,1,0:T(2,128)(2,1)}, bf16[4,4,256]{2,1,0:T(4,128)(2,1)}, f32[1,512]{1,0:T(1,128)S(1)}, f32[1,512]{1,0:T(1,128)S(1)}) custom-call(s32[2]{0:T(128)S(1)} %pad_add_fusion.refs_0_, bf16[272,512]{1,0:T(8,128)(2,1)S(1)} %collective-permute-done.refs_1_, ...), custom_call_target="tpu_custom_call", output_to_operand_aliasing={{0}: (9, {}), {1}: (10, {})} | custom-call | flops 1073741824 | bytes 5767168 | tf_op jit(solution)/shard_map/pallas_call | solution.py:183
  53.6 9.0 %collective-permute-start.12 = (f32[1,512]{1,0:T(1,128)S(1)}, f32[1,512]{1,0:T(1,128)S(1)}, u32[]{:S(2)}, u32[]{:S(2)}) collective-permute-start(f32[1,512]{1,0:T(1,128)S(1)} %multiply_add_fusion), channel_id=1, source_target_pairs={{0,8},{4,12},{8,0},{12,4},{1,9},{5,13},{9,1},{13,5},{2,10},{6,14},... | collective-permute-start | bytes 6152 | tf_op jit(solution)/shard_map/ppermute | solution.py:223
  62.6 0.9 %collective-permute-start.13 = (f32[1,512]{1,0:T(1,128)S(1)}, f32[1,512]{1,0:T(1,128)S(1)}, u32[]{:S(2)}, u32[]{:S(2)}) collective-permute-start(f32[1,512]{1,0:T(1,128)S(1)} %multiply_add_fusion), channel_id=1, source_target_pairs={{0,12},{4,8},{8,4},{12,0},{1,13},{5,9},{9,5},{13,1},{2,14},{6,10},... | collective-permute-start | bytes 6152 | tf_op jit(solution)/shard_map/ppermute | solution.py:223
  63.5 0.0 collective-permute-start.14
  63.5 0.7 collective-permute-done.12
  64.1 3.8 %collective-permute-done.13 = f32[1,512]{1,0:T(1,128)S(1)} collective-permute-done((f32[1,512]{1,0:T(1,128)S(1)}, f32[1,512]{1,0:T(1,128)S(1)}, u32[]{:S(2)}, u32[]{:S(2)}) %collective-permute-start.13) | collective-permute-done | bytes 2080 | tf_op jit(solution)/shard_map/ppermute | solution.py:223
  68.0 0.0 collective-permute-done.14
  68.0 0.7 select_select_fusion
  (17 shorter events, 0.1 us)
Async XLA Ops:
  0.6 22.9 %copy-start.5 = (bf16[4,256,4]{1,2,0:T(4,128)(2,1)S(1)}, bf16[4,256,4]{1,2,0:T(4,128)(2,1)}, u32[]{:S(2)}) copy-start(bf16[4,256,4]{1,2,0:T(4,128)(2,1)} %param.10) | copy-start | bytes 24580
  0.6 17.4 %copy-start.6 = (bf16[2048]{0:T(1024)(128)(2,1)S(1)}, bf16[2048]{0:T(1024)(128)(2,1)}, u32[]{:S(2)}) copy-start(bf16[2048]{0:T(1024)(128)(2,1)} %param.7) | copy-start | bytes 12292
  0.7 17.4 %copy-start.7 = (bf16[4,512]{1,0:T(4,128)(2,1)S(1)}, bf16[4,512]{1,0:T(4,128)(2,1)}, u32[]{:S(2)}) copy-start(bf16[4,512]{1,0:T(4,128)(2,1)} %param.11) | copy-start | bytes 12292
  0.7 22.8 %copy-start = (bf16[2048,512]{1,0:T(8,128)(2,1)S(1)}, bf16[2048,512]{1,0:T(8,128)(2,1)}, u32[]{:S(2)}) copy-start(bf16[2048,512]{1,0:T(8,128)(2,1)} %refs_6_.5) | copy-start | bytes 6291460
  2.8 10.2 %collective-permute-start.1 = (bf16[272,512]{1,0:T(8,128)(2,1)S(1)}, bf16[272,512]{1,0:T(8,128)(2,1)S(1)}, u32[]{:S(2)}, u32[]{:S(2)}) collective-permute-start(bf16[272,512]{1,0:T(8,128)(2,1)S(1)} %fusion.4), channel_id=1, source_target_pairs={{0,4},{4,0},{8,12},{12,8},{1,5},{5,1},{9,13},{13,9},{2,6},{6,2},{1... | collective-permute-start | bytes 835592 | tf_op jit(solution)/shard_map/ppermute | solution.py:223
  6.6 15.3 %collective-permute-start.7 = (bf16[272,512]{1,0:T(8,128)(2,1)}, bf16[272,512]{1,0:T(8,128)(2,1)S(1)}, u32[]{:S(2)}, u32[]{:S(2)}) collective-permute-start(bf16[272,512]{1,0:T(8,128)(2,1)} %fusion.5), channel_id=1, source_target_pairs={{0,12},{4,8},{8,4},{12,0},{1,13},{5,9},{9,5},{13,1},{2,14},{6,10},... | collective-permute-start | bytes 835592 | tf_op jit(solution)/shard_map/ppermute | solution.py:223
  12.9 10.5 %collective-permute-start.3 = (bf16[272,512]{1,0:T(8,128)(2,1)S(1)}, bf16[272,512]{1,0:T(8,128)(2,1)S(1)}, u32[]{:S(2)}, u32[]{:S(2)}) collective-permute-start(bf16[272,512]{1,0:T(8,128)(2,1)S(1)} %collective-permute-done.1.refs_1_), channel_id=1, source_target_pairs={{0,2},{1,3},{2,0},{3,1},{4,6},{5,7},{6,4},{7,5},{8,10},{9,11},{10,... | collective-permute-start | bytes 835592 | tf_op jit(solution)/shard_map/ppermute | solution.py:223
  14.4 22.4 %collective-permute-start = (bf16[272,512]{1,0:T(8,128)(2,1)S(1)}, bf16[272,512]{1,0:T(8,128)(2,1)S(1)}, u32[]{:S(2)}, u32[]{:S(2)}) collective-permute-start(bf16[272,512]{1,0:T(8,128)(2,1)S(1)} %fusion.3), channel_id=1, source_target_pairs={{0,8},{4,12},{8,0},{12,4},{1,9},{5,13},{9,1},{13,5},{2,10},{6,14},... | collective-permute-start | bytes 835592 | tf_op jit(solution)/shard_map/ppermute | solution.py:223
  18.0 14.3 %collective-permute-start.2 = (bf16[272,512]{1,0:T(8,128)(2,1)S(1)}, bf16[272,512]{1,0:T(8,128)(2,1)S(1)}, u32[]{:S(2)}, u32[]{:S(2)}) collective-permute-start(bf16[272,512]{1,0:T(8,128)(2,1)S(1)} %collective-permute-done.1.refs_1_), channel_id=1, source_target_pairs={{0,1},{1,0},{2,3},{3,2},{4,5},{5,4},{6,7},{7,6},{8,9},{9,8},{10,11... | collective-permute-start | bytes 835592 | tf_op jit(solution)/shard_map/ppermute | solution.py:223
  21.9 10.3 %collective-permute-start.9 = (bf16[272,512]{1,0:T(8,128)(2,1)S(1)}, bf16[272,512]{1,0:T(8,128)(2,1)S(1)}, u32[]{:S(2)}, u32[]{:S(2)}) collective-permute-start(bf16[272,512]{1,0:T(8,128)(2,1)S(1)} %collective-permute-done.7.refs_1_), channel_id=1, source_target_pairs={{0,2},{1,3},{2,0},{3,1},{4,6},{5,7},{6,4},{7,5},{8,10},{9,11},{10,... | collective-permute-start | bytes 835592 | tf_op jit(solution)/shard_map/ppermute | solution.py:223
  23.4 8.9 %collective-permute-start.4 = (bf16[272,512]{1,0:T(8,128)(2,1)S(1)}, bf16[272,512]{1,0:T(8,128)(2,1)S(1)}, u32[]{:S(2)}, u32[]{:S(2)}) collective-permute-start(bf16[272,512]{1,0:T(8,128)(2,1)S(1)} %collective-permute-done.3.refs_3_), channel_id=1, source_target_pairs={{0,1},{1,0},{2,3},{3,2},{4,5},{5,4},{6,7},{7,6},{8,9},{9,8},{10,11... | collective-permute-start | bytes 835592 | tf_op jit(solution)/shard_map/ppermute | solution.py:223
  23.5 1.6 %copy-start.1 = (bf16[2048,512]{1,0:T(8,128)(2,1)S(1)}, bf16[2048,512]{1,0:T(8,128)(2,1)}, u32[]{:S(2)}) copy-start(bf16[2048,512]{1,0:T(8,128)(2,1)} %refs_7_.5) | copy-start | bytes 6291460
  25.1 2.2 %copy-start.4 = (bf16[4,256,2048]{2,1,0:T(8,128)(2,1)S(1)}, bf16[4,256,2048]{2,1,0:T(8,128)(2,1)}, u32[]{:S(2)}) copy-start(bf16[4,256,2048]{2,1,0:T(8,128)(2,1)} %refs_1_.1) | copy-start | bytes 12582916
  27.3 5.0 %copy-start.2 = (bf16[2048,512]{1,0:T(8,128)(2,1)S(1)}, bf16[2048,512]{1,0:T(8,128)(2,1)}, u32[]{:S(2)}) copy-start(bf16[2048,512]{1,0:T(8,128)(2,1)} %refs_7_.5) | copy-start | bytes 6291460
  31.7 5.9 %collective-permute-start.8 = (bf16[272,512]{1,0:T(8,128)(2,1)S(1)}, bf16[272,512]{1,0:T(8,128)(2,1)S(1)}, u32[]{:S(2)}, u32[]{:S(2)}) collective-permute-start(bf16[272,512]{1,0:T(8,128)(2,1)S(1)} %collective-permute-done.7.refs_1_), channel_id=1, source_target_pairs={{0,1},{1,0},{2,3},{3,2},{4,5},{5,4},{6,7},{7,6},{8,9},{9,8},{10,11... | collective-permute-start | bytes 835592 | tf_op jit(solution)/shard_map/ppermute | solution.py:223
  32.2 5.4 %collective-permute-start.10 = (bf16[272,512]{1,0:T(8,128)(2,1)S(1)}, bf16[272,512]{1,0:T(8,128)(2,1)S(1)}, u32[]{:S(2)}, u32[]{:S(2)}) collective-permute-start(bf16[272,512]{1,0:T(8,128)(2,1)S(1)} %collective-permute-done.9.refs_3_), channel_id=1, source_target_pairs={{0,1},{1,0},{2,3},{3,2},{4,5},{5,4},{6,7},{7,6},{8,9},{9,8},{10,11... | collective-permute-start | bytes 835592 | tf_op jit(solution)/shard_map/ppermute | solution.py:223
  36.8 9.1 %collective-permute-start.6 = (bf16[272,512]{1,0:T(8,128)(2,1)S(1)}, bf16[272,512]{1,0:T(8,128)(2,1)S(1)}, u32[]{:S(2)}, u32[]{:S(2)}) collective-permute-start(bf16[272,512]{1,0:T(8,128)(2,1)S(1)} %collective-permute-done.refs_1_), channel_id=1, source_target_pairs={{0,2},{1,3},{2,0},{3,1},{4,6},{5,7},{6,4},{7,5},{8,10},{9,11},{10,... | collective-permute-start | bytes 835592 | tf_op jit(solution)/shard_map/ppermute | solution.py:223
  37.5 8.5 %collective-permute-start.5 = (bf16[272,512]{1,0:T(8,128)(2,1)S(1)}, bf16[272,512]{1,0:T(8,128)(2,1)S(1)}, u32[]{:S(2)}, u32[]{:S(2)}) collective-permute-start(bf16[272,512]{1,0:T(8,128)(2,1)S(1)} %collective-permute-done.refs_1_), channel_id=1, source_target_pairs={{0,1},{1,0},{2,3},{3,2},{4,5},{5,4},{6,7},{7,6},{8,9},{9,8},{10,11... | collective-permute-start | bytes 835592 | tf_op jit(solution)/shard_map/ppermute | solution.py:223
  45.9 1.6 %collective-permute-start.11 = (bf16[272,512]{1,0:T(8,128)(2,1)S(1)}, bf16[272,512]{1,0:T(8,128)(2,1)S(1)}, u32[]{:S(2)}, u32[]{:S(2)}) collective-permute-start(bf16[272,512]{1,0:T(8,128)(2,1)S(1)} %collective-permute-done.6.refs_3_), channel_id=1, source_target_pairs={{0,1},{1,0},{2,3},{3,2},{4,5},{5,4},{6,7},{7,6},{8,9},{9,8},{10,11... | collective-permute-start | bytes 835592 | tf_op jit(solution)/shard_map/ppermute | solution.py:223
  47.4 1.6 %copy-start.3 = (bf16[2048,512]{1,0:T(8,128)(2,1)S(1)}, bf16[2048,512]{1,0:T(8,128)(2,1)}, u32[]{:S(2)}) copy-start(bf16[2048,512]{1,0:T(8,128)(2,1)} %refs_7_.5) | copy-start | bytes 6291460
  53.6 10.6 %collective-permute-start.12 = (f32[1,512]{1,0:T(1,128)S(1)}, f32[1,512]{1,0:T(1,128)S(1)}, u32[]{:S(2)}, u32[]{:S(2)}) collective-permute-start(f32[1,512]{1,0:T(1,128)S(1)} %multiply_add_fusion), channel_id=1, source_target_pairs={{0,8},{4,12},{8,0},{12,4},{1,9},{5,13},{9,1},{13,5},{2,10},{6,14},... | collective-permute-start | bytes 6152 | tf_op jit(solution)/shard_map/ppermute | solution.py:223
  62.6 5.4 %collective-permute-start.13 = (f32[1,512]{1,0:T(1,128)S(1)}, f32[1,512]{1,0:T(1,128)S(1)}, u32[]{:S(2)}, u32[]{:S(2)}) collective-permute-start(f32[1,512]{1,0:T(1,128)S(1)} %multiply_add_fusion), channel_id=1, source_target_pairs={{0,12},{4,8},{8,4},{12,0},{1,13},{5,9},{9,5},{13,1},{2,14},{6,10},... | collective-permute-start | bytes 6152 | tf_op jit(solution)/shard_map/ppermute | solution.py:223
  63.5 4.5 %collective-permute-start.14 = (f32[1,512]{1,0:T(1,128)S(1)}, f32[1,512]{1,0:T(1,128)S(1)}, u32[]{:S(2)}, u32[]{:S(2)}) collective-permute-start(f32[1,512]{1,0:T(1,128)S(1)} %multiply_add_fusion), channel_id=1, source_target_pairs={{0,4},{4,0},{8,12},{12,8},{1,5},{5,1},{9,13},{13,9},{2,6},{6,2},{1... | collective-permute-start | bytes 6152 | tf_op jit(solution)/shard_map/ppermute | solution.py:223
